TPU v7x, 32 devices: a whole 2x2x4 slice. The times are simulated.
32 devices in a mesh: grp: 2 (over y), sp: 4 (over z), tp: 4 (over x, core).
Axes of the slice: x: 2, y: 2, z: 4, core: 2. Of those that a mesh axis runs over, the one named last changes fastest.
Arguments:
- residual_in: bfloat16 [2048, 2048], P(('grp', 'sp', 'tp')), parts along dimension 0, may hold values from -1.1953125 to 1.1953125
- query_small: bfloat16 [2048, 1024], P(('grp', 'sp'), 'tp'), parts along dimension 0, may hold values from -6 to 6
- query_large: bfloat16 [2048, 1024], P(('grp', 'sp'), 'tp'), parts along dimension 0, may hold values from -6 to 6
- key_small: bfloat16 [64, 2048], P(None, ('grp', 'sp')), parts along dimension 1, may hold values from -6 to 6
- key_large: bfloat16 [128, 2048], P(None, ('grp', 'sp')), parts along dimension 1, may hold values from -6 to 6
- value_small: bfloat16 [64, 2048], P(None, ('grp', 'sp')), parts along dimension 1, may hold values from -6 to 6
- value_large: bfloat16 [128, 2048], P(None, ('grp', 'sp')), parts along dimension 1, may hold values from -6 to 6
- forget_small: float32 [16, 2048], P('tp', ('grp', 'sp')), parts along dimension 1, may hold values from -148 to 0, as said below
- forget_large: float32 [8, 2048], P('tp', ('grp', 'sp')), parts along dimension 1, may hold values from -148 to 0, as said below
- project_small: bfloat16 [1024, 2048], P('tp'), may hold values from -0.125 to 0.125
- project_large: bfloat16 [1024, 2048], P('tp'), may hold values from -0.125 to 0.125
- norm_gain: bfloat16 [2048], replicated, may hold values from 0.099609375 to 1.8984375
- expert_gate: bfloat16 [16, 2048, 512], P(('sp', 'tp')), may hold values from -0.125 to 0.125
- expert_up: bfloat16 [16, 2048, 512], P(('sp', 'tp')), may hold values from -0.125 to 0.125
- expert_down: bfloat16 [16, 512, 2048], P(('sp', 'tp')), may hold values from -0.25 to 0.25
- routing: int32 [2048, 2], P(('grp', 'sp', 'tp')), parts along dimension 0, may hold values from 0 to 15, all different within a row; in each aligned block of 64 rows (0 to 63, 64 to 127, ...) at most 16 rows name the same one
- route_weight: float32 [2048, 2], P(('grp', 'sp', 'tp')), parts along dimension 0, may hold values from 0.2 to 1
Outputs:
- layer_out: bfloat16 [2048, 2048], P(('grp', 'sp', 'tp')), parts along dimension 0
There are 2 independent parts, one for each index of `grp`. A program takes and returns all parts, laid end to end along the dimension named above; an argument that names none is the same for every part. Nothing has to cross between parts.
Inputs may be any that keep to these rules, and one draw needn't show every extreme that they name: `forget_small`: each row never rises from one position to the next. `forget_large`: each row never rises from one position to the next. `routing`: each row names 2 different experts; in the rows of one device no expert is named by more than 16 rows, and in some devices' rows some expert is named by exactly 16.
All inputs are finite; a program needn't handle non-finite values.
Results may differ from a plain program's by a relative error of at most 0.018.
Values may be sent and summed in bfloat16 or wider, within the bound.
A program may use at most 64 MiB of HBM per device.

v0:
```python
import functools

import jax
import jax.numpy as jnp
from jax import lax
from jax.experimental import pallas as pl
from jax.experimental.pallas import tpu as pltpu
from jax.sharding import PartitionSpec as P

MESH = pl.DeviceIdType.MESH
F32 = jnp.float32
BF16 = jnp.bfloat16


def layer_kernel(
    dims,
    residual_in,
    query_small,
    query_large,
    key_small,
    key_large,
    value_small,
    value_large,
    forget_small,
    forget_large,
    norm_gain,
    routing,
    route_weight,
    project_small,
    project_large,
    expert_gate,
    expert_up,
    expert_down,
    out,
    kv,
    gates,
    heads_q_small,
    heads_q_large,
    top_ref,
    total_ref,
    acc_small,
    acc_large,
    attn,
    proj_w,
    gate_w,
    up_w,
    down_w,
    proj_f32,
    pair_out,
    pair_in,
    cross_out,
    cross_in,
    resid_ref,
    pick_ref,
    outgoing,
    arrived,
    scale_out,
    scale_in,
    result,
    returned,
    weight_sem,
    kv_send,
    kv_recv,
    gate_send,
    gate_recv,
    fwd_send,
    fwd_recv,
    pair_send,
    pair_recv,
    cross_send,
    cross_recv,
    disp_send,
    disp_recv,
    back_send,
    back_recv,
):
    n_sp, n_tp, cap, col_len = dims
    experts = n_sp * n_tp
    seq = lax.axis_index("sp")
    ten = lax.axis_index("tp")
    me = seq * n_tp + ten
    parity = lax.rem(ten, 2)
    partner = ten + 1 - 2 * parity
    tokens = query_small.shape[0]
    size_small, size_large = key_small.shape[0], key_large.shape[0]
    heads_small, heads_large = forget_small.shape[0], forget_large.shape[0]
    width_small = heads_small * size_small
    rows, width = residual_in.shape
    half_small, half_large = size_small // 2, size_large // 2
    cols = width // col_len
    half_groups = n_tp // 2

    loads = [
        pltpu.make_async_copy(project_small, proj_w.at[pl.ds(0, width_small)], weight_sem.at[0]),
        pltpu.make_async_copy(
            project_large,
            proj_w.at[pl.ds(width_small, heads_large * size_large)],
            weight_sem.at[1],
        ),
        pltpu.make_async_copy(expert_gate.at[0], gate_w, weight_sem.at[2]),
        pltpu.make_async_copy(expert_up.at[0], up_w, weight_sem.at[3]),
        pltpu.make_async_copy(expert_down.at[0], down_w, weight_sem.at[4]),
    ]
    for load in loads:
        load.start()

    barrier = pltpu.get_barrier_semaphore()

    def greet(i, carry):
        peer = lax.rem(me + i, experts)
        pl.semaphore_signal(
            barrier,
            inc=1,
            device_id={"sp": lax.div(peer, n_tp), "tp": lax.rem(peer, n_tp)},
            device_id_type=MESH,
        )
        return carry

    lax.fori_loop(1, experts, greet, 0)

    for half in range(2):
        base = 0
        for source, piece in (
            (key_small, half_small),
            (key_large, half_large),
            (value_small, half_small),
            (value_large, half_large),
        ):
            kv[seq, half, base : base + piece, :] = source[half * piece : (half + 1) * piece, :]
            base += piece
    gates[seq, :heads_small, :] = forget_small[...]
    gates[seq, heads_small : heads_small + heads_large, :] = forget_large[...]

    pl.semaphore_wait(barrier, experts - 1)

    def kv_copy(source, target, slot):
        return pltpu.make_async_remote_copy(
            src_ref=kv.at[source, parity],
            dst_ref=kv.at[source, parity],
            send_sem=kv_send.at[slot],
            recv_sem=kv_recv.at[source],
            device_id={"sp": target, "tp": ten},
            device_id_type=MESH,
        )

    def gate_copy(source, target, slot):
        return pltpu.make_async_remote_copy(
            src_ref=gates.at[source],
            dst_ref=gates.at[source],
            send_sem=gate_send.at[slot],
            recv_sem=gate_recv.at[source],
            device_id={"sp": target, "tp": ten},
            device_id_type=MESH,
        )

    def fwd_copy(source, half):
        return pltpu.make_async_remote_copy(
            src_ref=kv.at[source, half],
            dst_ref=kv.at[source, half],
            send_sem=fwd_send.at[source],
            recv_sem=fwd_recv.at[source],
            device_id={"sp": seq, "tp": partner},
            device_id_type=MESH,
        )

    def send_kv(target, carry):
        gate_copy(seq, target, target).start()
        kv_copy(seq, target, target).start()
        return carry

    lax.fori_loop(seq + 1, n_sp, send_kv, 0)

    lanes = lax.broadcasted_iota(jnp.int32, (rows, experts), 1)
    same = lax.broadcasted_iota(jnp.int32, (rows, rows), 0) == lax.broadcasted_iota(
        jnp.int32, (rows, rows), 1
    )

    def column(ref, k):
        return jnp.sum(
            jnp.where(same, ref[k : k + 1, :].astype(F32), 0.0), axis=1, keepdims=True
        )

    top_count = routing.shape[0]
    routes = [column(routing, k) for k in range(top_count)]
    hot = [(routes[k] == lanes.astype(F32)).astype(F32) for k in range(top_count)]
    named = sum(hot).astype(BF16)
    below = (
        lax.broadcasted_iota(jnp.int32, (rows, rows), 0)
        > lax.broadcasted_iota(jnp.int32, (rows, rows), 1)
    ).astype(F32)
    earlier = jnp.dot(below.astype(BF16), named, preferred_element_type=F32)
    places = lax.broadcasted_iota(jnp.int32, (rows, experts * cap), 1).astype(F32)
    for k in range(top_count):
        slot = jnp.sum(earlier * hot[k], axis=1, keepdims=True)
        place = routes[k] * cap + slot
        pick_ref[k * rows : (k + 1) * rows, :] = (places == place).astype(F32).astype(BF16)

    for h in range(heads_small):
        heads_q_small[h] = query_small[:, h * size_small : (h + 1) * size_small]
    for h in range(heads_large):
        heads_q_large[h] = query_large[:, h * size_large : (h + 1) * size_large]
    key_base = (0, half_small)
    value_base = (half_small + half_large, 2 * half_small + half_large)
    own_gates = gates[seq].T

    def attend(block, diagonal):
        block_gates = gates[block]
        for kind in range(2):
            heads, size, half, offset, q_ref, acc = (
                (heads_small, size_small, half_small, 0, heads_q_small, acc_small),
                (heads_large, size_large, half_large, heads_small, heads_q_large, acc_large),
            )[kind]
            kb, vb = key_base[kind], value_base[kind]
            keys = jnp.concatenate(
                [kv[block, 0, kb : kb + half, :], kv[block, 1, kb : kb + half, :]], axis=0
            )
            values = jnp.concatenate(
                [kv[block, 0, vb : vb + half, :], kv[block, 1, vb : vb + half, :]], axis=0
            )
            for h in range(heads):
                g = offset + h
                scores = jnp.dot(q_ref[h], keys, preferred_element_type=F32) * size ** (-0.5)
                scores = scores + own_gates[:, g : g + 1] - block_gates[g : g + 1, :]
                if diagonal:
                    q_pos = lax.broadcasted_iota(jnp.int32, (tokens, tokens), 0)
                    k_pos = lax.broadcasted_iota(jnp.int32, (tokens, tokens), 1)
                    scores = jnp.where(q_pos >= k_pos, scores, -jnp.inf)
                block_top = jnp.max(scores, axis=1, keepdims=True)
                top = block_top if diagonal else jnp.maximum(top_ref[g], block_top)
                weights = jnp.exp(scores - top)
                total = jnp.sum(weights, axis=1, keepdims=True)
                mixed = lax.dot_general(
                    weights.astype(BF16),
                    values,
                    (((1,), (1,)), ((), ())),
                    preferred_element_type=F32,
                )
                if not diagonal:
                    factor = jnp.exp(top_ref[g] - top)
                    total = total_ref[g] * factor + total
                    mixed = acc[h] * factor + mixed
                top_ref[g] = top
                total_ref[g] = total
                acc[h] = mixed

    def pass_on(block):
        kv_copy(block, seq, block).wait_recv()
        fwd_copy(block, parity).start()

    @pl.when(seq > 0)
    def _():
        pass_on(seq - 1)

    attend(seq, True)

    def earlier_block(i, carry):
        block = seq - 1 - i

        @pl.when(block > 0)
        def _():
            pass_on(block - 1)

        fwd_copy(block, 1 - parity).wait_recv()
        gate_copy(block, seq, block).wait_recv()
        attend(block, False)
        return carry

    lax.fori_loop(0, seq, earlier_block, 0)

    for h in range(heads_small):
        attn[:, h * size_small : (h + 1) * size_small] = (acc_small[h] / total_ref[h]).astype(BF16)
    for h in range(heads_large):
        first = width_small + h * size_large
        attn[:, first : first + size_large] = (
            acc_large[h] / total_ref[heads_small + h]
        ).astype(BF16)

    def row_ds(group, par):
        return pl.ds(pl.multiple_of((2 * group + par) * rows, rows), rows)

    def pair_copy(c):
        return pltpu.make_async_remote_copy(
            src_ref=pair_out.at[c],
            dst_ref=pair_in.at[c],
            send_sem=pair_send.at[c],
            recv_sem=pair_recv.at[c],
            device_id={"sp": seq, "tp": partner},
            device_id_type=MESH,
        )

    def cross_copy(c, group, source, slot):
        return pltpu.make_async_remote_copy(
            src_ref=cross_out.at[c, group],
            dst_ref=cross_in.at[c, source],
            send_sem=cross_send.at[c, slot],
            recv_sem=cross_recv.at[c, source],
            device_id={"sp": seq, "tp": 2 * group + parity},
            device_id_type=MESH,
        )

    my_group = lax.div(ten, 2)
    for load in loads[:2]:
        load.wait()
    for c in range(cols):
        part = jnp.dot(
            attn[...], proj_w[:, c * col_len : (c + 1) * col_len], preferred_element_type=F32
        )
        proj_f32[c] = part
        for group in range(half_groups):
            pair_out[c, group] = proj_f32[c, row_ds(group, 1 - parity), :].astype(BF16)
        pair_copy(c).start()
    for c in range(cols):
        pair_copy(c).wait_recv()
        for hop in range(1, half_groups):
            group = lax.rem(my_group + hop, half_groups)
            cross_out[c, group] = (
                proj_f32[c, row_ds(group, parity), :] + pair_in[c, group].astype(F32)
            ).astype(BF16)
            cross_copy(c, group, my_group, hop).start()
    def slot_ds(peer):
        return pl.ds(pl.multiple_of(peer * cap, cap), cap)

    def exchange(source_ref, target_ref, send, recv, peer, sender):
        return pltpu.make_async_remote_copy(
            src_ref=source_ref.at[slot_ds(peer)],
            dst_ref=target_ref.at[slot_ds(sender)],
            send_sem=send.at[peer],
            recv_sem=recv.at[sender],
            device_id={"sp": lax.div(peer, n_tp), "tp": lax.rem(peer, n_tp)},
            device_id_type=MESH,
        )

    def part_copy(c, peer, sender):
        if c < cols:
            source_ref, target_ref = outgoing.at[c], arrived.at[c]
        else:
            source_ref, target_ref = scale_out, scale_in
        return exchange(source_ref, target_ref, disp_send.at[c], disp_recv.at[c], peer, sender)

    def for_members(plane, action):
        def one(j, carry):
            peer = plane * n_tp + lax.rem(ten + j, n_tp)

            @pl.when(peer != me)
            def _():
                action(peer)

            return carry

        lax.fori_loop(0, n_tp, one, 0)

    slots = experts * cap
    block_rows = min(256, slots)

    def place_rows(values, c):
        for b in range(slots // block_rows):
            span = slice(b * block_rows, (b + 1) * block_rows)
            chosen = pick_ref[:rows, span]
            for k in range(1, top_count):
                chosen = chosen + pick_ref[k * rows : (k + 1) * rows, span]
            placed = lax.dot_general(
                chosen, values, (((0,), (0,)), ((), ())), preferred_element_type=F32
            ).astype(BF16)
            if c < cols:
                outgoing[c, span, :] = placed
            else:
                scale_out[span, :] = placed

        def dispatch(i, carry):
            for_members(
                lax.rem(seq + n_sp - i, n_sp), lambda peer: part_copy(c, peer, me).start()
            )
            return carry

        lax.fori_loop(0, n_sp, dispatch, 0)

    squares = jnp.zeros((rows, 1), F32)
    gain = norm_gain[...].astype(F32).reshape(1, width)
    for c in range(cols):
        span = slice(c * col_len, (c + 1) * col_len)
        value = proj_f32[c, row_ds(my_group, parity), :] + pair_in[c, my_group].astype(F32)
        for hop in range(1, half_groups):
            source = lax.rem(my_group + hop, half_groups)
            cross_copy(c, source, source, hop).wait_recv()
            value = value + cross_in[c, source].astype(F32)
        value = value + residual_in[:, span].astype(F32)
        resid_ref[:, span] = value
        squares = squares + jnp.sum(value * value, axis=1, keepdims=True)
        place_rows((value * gain[:, span]).astype(BF16), c)
    scale = lax.rsqrt(squares * (1.0 / width) + 1e-06)
    first = scale.astype(BF16).astype(F32)
    second = (scale - first).astype(BF16).astype(F32)
    third = scale - first - second
    lane = lax.broadcasted_iota(jnp.int32, (rows, 128), 1)
    parts = jnp.where(lane == 0, first, jnp.where(lane == 1, second, jnp.where(lane == 2, third, 0.0)))
    place_rows(parts.astype(BF16), cols)
    for c in range(cols):
        arrived[c, slot_ds(me), :] = outgoing[c, slot_ds(me), :]
    scale_in[slot_ds(me), :] = scale_out[slot_ds(me), :]
    for load in loads[2:]:
        load.wait()

    group_rows = n_tp * cap

    def serve(i, carry):
        plane = lax.rem(seq + i, n_sp)
        span = pl.ds(pl.multiple_of(plane * group_rows, group_rows), group_rows)
        gate_part = jnp.zeros((group_rows, gate_w.shape[1]), F32)
        up_part = jnp.zeros((group_rows, gate_w.shape[1]), F32)
        for c in range(cols):
            for_members(plane, lambda peer: part_copy(c, me, peer).wait_recv())
            came = arrived[c, span, :]
            depth = slice(c * col_len, (c + 1) * col_len)
            gate_part = gate_part + jnp.dot(came, gate_w[depth, :], preferred_element_type=F32)
            up_part = up_part + jnp.dot(came, up_w[depth, :], preferred_element_type=F32)
        for_members(plane, lambda peer: part_copy(cols, me, peer).wait_recv())
        row_scale = jnp.sum(scale_in[span, :].astype(F32), axis=1, keepdims=True)
        gate_part, up_part = gate_part * row_scale, up_part * row_scale
        hidden = (gate_part / (1.0 + jnp.exp(-gate_part)) * up_part).astype(BF16)
        result[span, :] = jnp.dot(hidden, down_w[...], preferred_element_type=F32).astype(BF16)
        for_members(
            plane,
            lambda peer: exchange(result, returned, back_send, back_recv, peer, me).start(),
        )
        return carry

    lax.fori_loop(0, n_sp, serve, 0)
    returned[slot_ds(me), :] = result[slot_ds(me), :]

    def collect(i, carry):
        peer = lax.rem(me + i, experts)
        exchange(result, returned, back_send, back_recv, me, peer).wait_recv()
        return carry

    lax.fori_loop(1, experts, collect, 0)
    for c in range(cols):
        span = slice(c * col_len, (c + 1) * col_len)
        picked = jnp.dot(pick_ref[...], returned[:, span], preferred_element_type=F32)
        value = resid_ref[:, span]
        for k in range(top_count):
            value = value + picked[k * rows : (k + 1) * rows] * column(route_weight, k)
        out[:, span] = value.astype(BF16)

    def sent_kv(target, carry):
        gate_copy(seq, target, target).wait_send()
        kv_copy(seq, target, target).wait_send()
        return carry

    lax.fori_loop(seq + 1, n_sp, sent_kv, 0)

    def sent_fwd(block, carry):
        fwd_copy(block, parity).wait_send()
        return carry

    lax.fori_loop(0, seq, sent_fwd, 0)
    for c in range(cols):
        pair_copy(c).wait_send()
        for hop in range(1, half_groups):
            group = lax.rem(my_group + hop, half_groups)
            cross_copy(c, group, my_group, hop).wait_send()

    def sent_rows(i, carry):
        peer = lax.rem(me + i, experts)
        for c in range(cols + 1):
            part_copy(c, peer, me).wait_send()
        exchange(result, returned, back_send, back_recv, peer, me).wait_send()
        return carry

    lax.fori_loop(1, experts, sent_rows, 0)


def shards(
    residual_in,
    query_small,
    query_large,
    key_small,
    key_large,
    value_small,
    value_large,
    forget_small,
    forget_large,
    project_small,
    project_large,
    norm_gain,
    expert_gate,
    expert_up,
    expert_down,
    routing,
    route_weight,
):
    n_sp, n_tp = lax.axis_size("sp"), lax.axis_size("tp")
    experts = n_sp * n_tp
    rows, width = residual_in.shape
    top_count = routing.shape[1]
    tokens = query_small.shape[0]
    size_small, size_large = key_small.shape[0], key_large.shape[0]
    heads_small, heads_large = forget_small.shape[0], forget_large.shape[0]
    heads = heads_small + heads_large
    capacity = max(2, 2 * rows * top_count // experts)
    cap = -(-capacity // 16) * 16
    col_len = min(width, 512)
    cols = width // col_len
    hidden = expert_gate.shape[2]
    attn_width = heads_small * size_small + heads_large * size_large
    half_groups = n_tp // 2
    slots = experts * cap
    vmem, dma = pltpu.VMEM, pltpu.SemaphoreType.DMA
    return pl.pallas_call(
        functools.partial(layer_kernel, (n_sp, n_tp, cap, col_len)),
        out_shape=jax.ShapeDtypeStruct((rows, width), BF16),
        in_specs=[pl.BlockSpec(memory_space=pltpu.VMEM)] * 12
        + [pl.BlockSpec(memory_space=pl.ANY)] * 5,
        out_specs=pl.BlockSpec(memory_space=pltpu.VMEM),
        scratch_shapes=[
            vmem((n_sp, 2, size_small + size_large, tokens), BF16),
            vmem((n_sp, -(-heads // 8) * 8, tokens), F32),
            vmem((heads_small, tokens, size_small), BF16),
            vmem((heads_large, tokens, size_large), BF16),
            vmem((heads, tokens, 1), F32),
            vmem((heads, tokens, 1), F32),
            vmem((heads_small, tokens, size_small), F32),
            vmem((heads_large, tokens, size_large), F32),
            vmem((tokens, attn_width), BF16),
            vmem((attn_width, width), BF16),
            vmem((width, hidden), BF16),
            vmem((width, hidden), BF16),
            vmem((hidden, width), BF16),
            vmem((cols, tokens, col_len), F32),
            vmem((cols, half_groups, rows, col_len), BF16),
            vmem((cols, half_groups, rows, col_len), BF16),
            vmem((cols, half_groups, rows, col_len), BF16),
            vmem((cols, half_groups, rows, col_len), BF16),
            vmem((rows, width), F32),
            vmem((top_count * rows, slots), BF16),
            vmem((cols, slots, col_len), BF16),
            vmem((cols, slots, col_len), BF16),
            vmem((slots, 128), BF16),
            vmem((slots, 128), BF16),
            vmem((slots, width), BF16),
            vmem((slots, width), BF16),
            dma((5,)),
            dma((n_sp,)),
            dma((n_sp,)),
            dma((n_sp,)),
            dma((n_sp,)),
            dma((n_sp,)),
            dma((n_sp,)),
            dma((cols,)),
            dma((cols,)),
            dma((cols, half_groups)),
            dma((cols, half_groups)),
            dma((cols + 1, experts)),
            dma((cols + 1, experts)),
            dma((experts,)),
            dma((experts,)),
        ],
        compiler_params=pltpu.CompilerParams(
            collective_id=0, has_side_effects=True, vmem_limit_bytes=60 * 1024 * 1024
        ),
    )(
        residual_in,
        query_small,
        query_large,
        key_small,
        key_large,
        value_small,
        value_large,
        forget_small,
        forget_large,
        norm_gain,
        routing.T,
        route_weight.T,
        project_small,
        project_large,
        expert_gate,
        expert_up,
        expert_down,
    )


def solution(mesh):
    in_specs = (
        P(("grp", "sp", "tp"), None),
        P(("grp", "sp"), "tp"),
        P(("grp", "sp"), "tp"),
        P(None, ("grp", "sp")),
        P(None, ("grp", "sp")),
        P(None, ("grp", "sp")),
        P(None, ("grp", "sp")),
        P("tp", ("grp", "sp")),
        P("tp", ("grp", "sp")),
        P("tp", None),
        P("tp", None),
        P(),
        P(("sp", "tp"), None, None),
        P(("sp", "tp"), None, None),
        P(("sp", "tp"), None, None),
        P(("grp", "sp", "tp"), None),
        P(("grp", "sp", "tp"), None),
    )
    out_specs = P(("grp", "sp", "tp"), None)
    return jax.shard_map(shards, mesh=mesh, in_specs=in_specs, out_specs=out_specs, check_vma=False)
```

profile of v0, /device:TPU:13, one launch (start us, length us, event | category | flops | bytes accessed | tf_op | source)
XLA Modules:
  0.0 82.2 jit_solution(10460240546270397565)
XLA Ops:
  0.0 80.5 %shard_map.163 = bf16[64,2048]{1,0:T(8,128)(2,1)} custom-call(bf16[64,2048]{1,0:T(8,128)(2,1)} %residual_in.1, bf16[256,256]{1,0:T(8,128)(2,1)} %query_small.1, bf16[256,256]{1,0:T(8,128)(2,1)} %query_large.1, bf16[64,256]{1,0:T(8,128)(2,1)} %key_small.1, bf16[128,256]{1,0:T(8,128)(2,1)} %key_large.1, bf16[64,256]{1,0:T(8,128)(2,1)} %value_small.1, ...), custom_call_target="tpu_custom_call" | custom-call | tf_op jit(solution)/shard_map/pallas_call | solution.py:508
  80.5 1.7 %copy.19 = bf16[64,2048]{1,0:T(8,128)(2,1)} copy(bf16[64,2048]{1,0:T(8,128)(2,1)} %shard_map.163) | data formatting | bytes 524288
where the time goes:
time: 82.3 us; the launch traced here: 82.2 us
  Pallas kernels  80.5 us (98%)
  local copies, waits for them, and re-layouts  1.67 us (2%)
    pallas_call x1, Pallas kernels, shards(): pl.pallas_call(functools.partial(layer_kernel, (n_sp, n_tp, cap, col_len)...  80.5 us
    unnamed x1, local copies, waits for them, and re-layouts  1.67 us

commit v1 on v0

--- a/solution.py
+++ b/solution.py
@@ -1,4 +1,5 @@
 import functools
+import math
 
 import jax
 import jax.numpy as jnp
@@ -34,12 +35,13 @@
     out,
     kv,
     gates,
-    heads_q_small,
-    heads_q_large,
+    turned_q_small,
+    turned_q_large,
     top_ref,
     total_ref,
     acc_small,
     acc_large,
+    attn_t,
     attn,
     proj_w,
     gate_w,
@@ -130,6 +132,11 @@
             base += piece
     gates[seq, :heads_small, :] = forget_small[...]
     gates[seq, heads_small : heads_small + heads_large, :] = forget_large[...]
+    gate_rows = gates.shape[1]
+    if gate_rows > heads_small + heads_large:
+        gates[seq, heads_small + heads_large :, :] = jnp.zeros(
+            (gate_rows - heads_small - heads_large, tokens), F32
+        )
 
     pl.semaphore_wait(barrier, experts - 1)
 
@@ -195,64 +202,85 @@
         place = routes[k] * cap + slot
         pick_ref[k * rows : (k + 1) * rows, :] = (places == place).astype(F32).astype(BF16)
 
-    for h in range(heads_small):
-        heads_q_small[h] = query_small[:, h * size_small : (h + 1) * size_small]
-    for h in range(heads_large):
-        heads_q_large[h] = query_large[:, h * size_large : (h + 1) * size_large]
+    extra_rows = turned_q_small.shape[1] - size_small
+
+    def fold(size):
+        power = 2.0 ** math.floor(math.log2(size**-0.5))
+        return power, size**-0.5 / power
+
+    extra_row = lax.broadcasted_iota(jnp.int32, (extra_rows, tokens), 0)
+    for kind in range(2):
+        heads, size, offset, source, q_ref = (
+            (heads_small, size_small, 0, query_small, turned_q_small),
+            (heads_large, size_large, heads_small, query_large, turned_q_large),
+        )[kind]
+        turned = (source[...] * fold(size)[0]).astype(BF16).T
+        for h in range(heads):
+            chosen = (lax.rem(extra_row, gate_rows) == offset + h) & (extra_row < 3 * gate_rows)
+            q_ref[h, :size, :] = turned[h * size : (h + 1) * size, :]
+            q_ref[h, size:, :] = jnp.where(chosen, 1.0, 0.0).astype(BF16)
     key_base = (0, half_small)
     value_base = (half_small + half_large, 2 * half_small + half_large)
-    own_gates = gates[seq].T
 
     def attend(block, diagonal):
         block_gates = gates[block]
+        if diagonal:
+            k_pos = lax.broadcasted_iota(jnp.int32, (tokens, tokens), 0)
+            q_pos = lax.broadcasted_iota(jnp.int32, (tokens, tokens), 1)
+            seen = q_pos >= k_pos
         for kind in range(2):
             heads, size, half, offset, q_ref, acc = (
-                (heads_small, size_small, half_small, 0, heads_q_small, acc_small),
-                (heads_large, size_large, half_large, heads_small, heads_q_large, acc_large),
+                (heads_small, size_small, half_small, 0, turned_q_small, acc_small),
+                (heads_large, size_large, half_large, heads_small, turned_q_large, acc_large),
             )[kind]
             kb, vb = key_base[kind], value_base[kind]
+            rest = fold(size)[1]
+            shift = block_gates * (-1.0 / rest)
+            first = shift.astype(BF16).astype(F32)
+            second = (shift - first).astype(BF16).astype(F32)
+            pieces = [first, second, shift - first - second]
+            if extra_rows > 3 * gate_rows:
+                pieces.append(jnp.zeros((extra_rows - 3 * gate_rows, tokens), F32))
             keys = jnp.concatenate(
-                [kv[block, 0, kb : kb + half, :], kv[block, 1, kb : kb + half, :]], axis=0
-            )
+                [
+                    kv[block, 0, kb : kb + half, :],
+                    kv[block, 1, kb : kb + half, :],
+                    jnp.concatenate(pieces, axis=0).astype(BF16),
+                ],
+                axis=0,
+            ).T
             values = jnp.concatenate(
                 [kv[block, 0, vb : vb + half, :], kv[block, 1, vb : vb + half, :]], axis=0
             )
             for h in range(heads):
-                g = offset + h
-                scores = jnp.dot(q_ref[h], keys, preferred_element_type=F32) * size ** (-0.5)
-                scores = scores + own_gates[:, g : g + 1] - block_gates[g : g + 1, :]
+                g = slice(offset + h, offset + h + 1)
+                scores = jnp.dot(keys, q_ref[h], preferred_element_type=F32)
                 if diagonal:
-                    q_pos = lax.broadcasted_iota(jnp.int32, (tokens, tokens), 0)
-                    k_pos = lax.broadcasted_iota(jnp.int32, (tokens, tokens), 1)
-                    scores = jnp.where(q_pos >= k_pos, scores, -jnp.inf)
-                block_top = jnp.max(scores, axis=1, keepdims=True)
-                top = block_top if diagonal else jnp.maximum(top_ref[g], block_top)
-                weights = jnp.exp(scores - top)
-                total = jnp.sum(weights, axis=1, keepdims=True)
-                mixed = lax.dot_general(
-                    weights.astype(BF16),
-                    values,
-                    (((1,), (1,)), ((), ())),
-                    preferred_element_type=F32,
-                )
+                    scores = jnp.where(seen, scores, -jnp.inf)
+                block_top = jnp.max(scores, axis=0, keepdims=True)
+                top = block_top if diagonal else jnp.maximum(top_ref[g, :], block_top)
+                below_top = scores - top
+                weights = jnp.exp(below_top if rest == 1.0 else below_top * rest)
+                total = jnp.sum(weights, axis=0, keepdims=True)
+                mixed = jnp.dot(values, weights.astype(BF16), preferred_element_type=F32)
                 if not diagonal:
-                    factor = jnp.exp(top_ref[g] - top)
-                    total = total_ref[g] * factor + total
+                    factor = jnp.exp((top_ref[g, :] - top) * rest)
+                    total = total_ref[g, :] * factor + total
                     mixed = acc[h] * factor + mixed
-                top_ref[g] = top
-                total_ref[g] = total
+                top_ref[g, :] = top
+                total_ref[g, :] = total
                 acc[h] = mixed
 
     def pass_on(block):
         kv_copy(block, seq, block).wait_recv()
         fwd_copy(block, parity).start()
 
+    attend(seq, True)
+
     @pl.when(seq > 0)
     def _():
         pass_on(seq - 1)
 
-    attend(seq, True)
-
     def earlier_block(i, carry):
         block = seq - 1 - i
 
@@ -268,12 +296,16 @@
     lax.fori_loop(0, seq, earlier_block, 0)
 
     for h in range(heads_small):
-        attn[:, h * size_small : (h + 1) * size_small] = (acc_small[h] / total_ref[h]).astype(BF16)
+        attn_t[h * size_small : (h + 1) * size_small, :] = (
+            acc_small[h] * (1.0 / total_ref[h : h + 1, :])
+        ).astype(BF16)
     for h in range(heads_large):
         first = width_small + h * size_large
-        attn[:, first : first + size_large] = (
-            acc_large[h] / total_ref[heads_small + h]
+        g = heads_small + h
+        attn_t[first : first + size_large, :] = (
+            acc_large[h] * (1.0 / total_ref[g : g + 1, :])
         ).astype(BF16)
+    attn[...] = attn_t[...].T
 
     def row_ds(group, par):
         return pl.ds(pl.multiple_of((2 * group + par) * rows, rows), rows)
@@ -496,6 +528,8 @@
     size_small, size_large = key_small.shape[0], key_large.shape[0]
     heads_small, heads_large = forget_small.shape[0], forget_large.shape[0]
     heads = heads_small + heads_large
+    gate_rows = -(-heads // 8) * 8
+    extra_rows = -(-3 * gate_rows // 16) * 16
     capacity = max(2, 2 * rows * top_count // experts)
     cap = -(-capacity // 16) * 16
     col_len = min(width, 512)
@@ -513,13 +547,14 @@
         out_specs=pl.BlockSpec(memory_space=pltpu.VMEM),
         scratch_shapes=[
             vmem((n_sp, 2, size_small + size_large, tokens), BF16),
-            vmem((n_sp, -(-heads // 8) * 8, tokens), F32),
-            vmem((heads_small, tokens, size_small), BF16),
-            vmem((heads_large, tokens, size_large), BF16),
-            vmem((heads, tokens, 1), F32),
-            vmem((heads, tokens, 1), F32),
-            vmem((heads_small, tokens, size_small), F32),
-            vmem((heads_large, tokens, size_large), F32),
+            vmem((n_sp, gate_rows, tokens), F32),
+            vmem((heads_small, size_small + extra_rows, tokens), BF16),
+            vmem((heads_large, size_large + extra_rows, tokens), BF16),
+            vmem((gate_rows, tokens), F32),
+            vmem((gate_rows, tokens), F32),
+            vmem((heads_small, size_small, tokens), F32),
+            vmem((heads_large, size_large, tokens), F32),
+            vmem((attn_width, tokens), BF16),
             vmem((tokens, attn_width), BF16),
             vmem((attn_width, width), BF16),
             vmem((width, hidden), BF16),

time: 82.3 us -> 81.3 us (0.988)
  Pallas kernels: 80.5 us -> 79.5 us
    pallas_call x1, Pallas kernels: 80.5 us -> 79.5 us  [shards(): pl.pallas_call(functools.partial(layer_kernel, (n_sp, n_tp, cap, col_len)...]
where the time goes in v1:
time: 81.3 us; the launch traced here: 81.1 us
  Pallas kernels  79.5 us (98%)
  local copies, waits for them, and re-layouts  1.67 us (2%)
    pallas_call x1, Pallas kernels, shards(): pl.pallas_call(functools.partial(layer_kernel, (n_sp, n_tp, cap, col_len)...  79.5 us
    unnamed x1, local copies, waits for them, and re-layouts  1.67 us

profile of v1, /device:TPU:13, one launch (start us, length us, event | category | flops | bytes accessed | tf_op | source)
XLA Modules:
  0.0 81.1 jit_solution(2978265883477558441)
XLA Ops:
  0.0 79.5 %shard_map.163 = bf16[64,2048]{1,0:T(8,128)(2,1)} custom-call(bf16[64,2048]{1,0:T(8,128)(2,1)} %residual_in.1, bf16[256,256]{1,0:T(8,128)(2,1)} %query_small.1, bf16[256,256]{1,0:T(8,128)(2,1)} %query_large.1, bf16[64,256]{1,0:T(8,128)(2,1)} %key_small.1, bf16[128,256]{1,0:T(8,128)(2,1)} %key_large.1, bf16[64,256]{1,0:T(8,128)(2,1)} %value_small.1, ...), custom_call_target="tpu_custom_call" | custom-call | tf_op jit(solution)/shard_map/pallas_call | solution.py:542
  79.5 1.7 %copy.19 = bf16[64,2048]{1,0:T(8,128)(2,1)} copy(bf16[64,2048]{1,0:T(8,128)(2,1)} %shard_map.163) | data formatting | bytes 524288

commit v2 on v1

v2 whole, which is shorter than its diff:
```python
import functools
import math

import jax
import jax.numpy as jnp
from jax import lax
from jax.experimental import pallas as pl
from jax.experimental.pallas import tpu as pltpu
from jax.sharding import PartitionSpec as P

MESH = pl.DeviceIdType.MESH
F32 = jnp.float32
BF16 = jnp.bfloat16


def layer_kernel(dims, *refs):
    (
        residual_in,
        query_small,
        query_large,
        key_small,
        key_large,
        value_small,
        value_large,
        forget_small,
        forget_large,
        norm_gain,
        routing,
        route_weight,
        project_small,
        project_large,
        expert_gate,
        expert_up,
        expert_down,
        out,
        kv,
        gates,
        turned_q_small,
        turned_q_large,
        top_ref,
        total_ref,
        acc_small,
        acc_large,
        attn_t,
        attn,
        proj_w,
        gate_w,
        up_w,
        down_w,
        proj_f32,
        pair_out,
        pair_in,
        cross_out,
        cross_in,
        resid_ref,
        weight_sem,
        kv_send,
        kv_recv,
        gate_send,
        gate_recv,
        fwd_send,
        fwd_recv,
        pair_send,
        pair_recv,
        cross_send,
        cross_recv,
        *tail,
    ) = refs
    n_sp, n_tp, cap, col_len, lined = dims
    experts = n_sp * n_tp
    seq = lax.axis_index("sp")
    ten = lax.axis_index("tp")
    me = seq * n_tp + ten
    parity = lax.rem(ten, 2)
    partner = ten + 1 - 2 * parity
    tokens = query_small.shape[0]
    size_small, size_large = key_small.shape[0], key_large.shape[0]
    heads_small, heads_large = forget_small.shape[0], forget_large.shape[0]
    width_small = heads_small * size_small
    rows, width = residual_in.shape
    piece_small, piece_large = size_small // n_tp, size_large // n_tp
    cols = width // col_len
    half_groups = n_tp // 2

    loads = [
        pltpu.make_async_copy(project_small, proj_w.at[pl.ds(0, width_small)], weight_sem.at[0]),
        pltpu.make_async_copy(
            project_large,
            proj_w.at[pl.ds(width_small, heads_large * size_large)],
            weight_sem.at[1],
        ),
        pltpu.make_async_copy(expert_gate.at[0], gate_w, weight_sem.at[2]),
        pltpu.make_async_copy(expert_up.at[0], up_w, weight_sem.at[3]),
        pltpu.make_async_copy(expert_down.at[0], down_w, weight_sem.at[4]),
    ]
    for load in loads:
        load.start()

    barrier = pltpu.get_barrier_semaphore()

    def greet(peer_sp, peer_tp):
        pl.semaphore_signal(
            barrier, inc=1, device_id={"sp": peer_sp, "tp": peer_tp}, device_id_type=MESH
        )

    if lined:
        for i in range(1, n_tp):
            greet(seq, lax.rem(ten + i, n_tp))
        for i in range(1, n_sp):
            greet(lax.rem(seq + i, n_sp), ten)
    else:

        def greet_all(i, carry):
            peer = lax.rem(me + i, experts)
            greet(lax.div(peer, n_tp), lax.rem(peer, n_tp))
            return carry

        lax.fori_loop(1, experts, greet_all, 0)

    for p in range(n_tp):
        base = 0
        for source, piece in (
            (key_small, piece_small),
            (key_large, piece_large),
            (value_small, piece_small),
            (value_large, piece_large),
        ):
            kv[seq, p, base : base + piece, :] = source[p * piece : (p + 1) * piece, :]
            base += piece
    gates[seq, :heads_small, :] = forget_small[...]
    gates[seq, heads_small : heads_small + heads_large, :] = forget_large[...]
    gate_rows = gates.shape[1]
    if gate_rows > heads_small + heads_large:
        gates[seq, heads_small + heads_large :, :] = jnp.zeros(
            (gate_rows - heads_small - heads_large, tokens), F32
        )

    pl.semaphore_wait(barrier, n_tp + n_sp - 2 if lined else experts - 1)

    def kv_copy(source, target, slot):
        return pltpu.make_async_remote_copy(
            src_ref=kv.at[source, ten],
            dst_ref=kv.at[source, ten],
            send_sem=kv_send.at[slot],
            recv_sem=kv_recv.at[source],
            device_id={"sp": target, "tp": ten},
            device_id_type=MESH,
        )

    def gate_copy(source, target, slot):
        return pltpu.make_async_remote_copy(
            src_ref=gates.at[source],
            dst_ref=gates.at[source],
            send_sem=gate_send.at[slot],
            recv_sem=gate_recv.at[source],
            device_id={"sp": target, "tp": ten},
            device_id_type=MESH,
        )

    def fwd_copy(source, piece, peer):
        return pltpu.make_async_remote_copy(
            src_ref=kv.at[source, piece],
            dst_ref=kv.at[source, piece],
            send_sem=fwd_send.at[source, peer],
            recv_sem=fwd_recv.at[source, piece],
            device_id={"sp": seq, "tp": peer},
            device_id_type=MESH,
        )

    def for_mates(action):
        for i in range(1, n_tp):
            action(lax.rem(ten + i, n_tp))

    def send_kv(target, carry):
        gate_copy(seq, target, target).start()
        kv_copy(seq, target, target).start()
        return carry

    lax.fori_loop(seq + 1, n_sp, send_kv, 0)

    lanes = lax.broadcasted_iota(jnp.int32, (rows, experts), 1)
    same = lax.broadcasted_iota(jnp.int32, (rows, rows), 0) == lax.broadcasted_iota(
        jnp.int32, (rows, rows), 1
    )

    def column(ref, k):
        return jnp.sum(
            jnp.where(same, ref[k : k + 1, :].astype(F32), 0.0), axis=1, keepdims=True
        )

    top_count = routing.shape[0]
    routes = [column(routing, k) for k in range(top_count)]
    hot = [(routes[k] == lanes.astype(F32)).astype(F32) for k in range(top_count)]
    named = sum(hot).astype(BF16)
    below = (
        lax.broadcasted_iota(jnp.int32, (rows, rows), 0)
        > lax.broadcasted_iota(jnp.int32, (rows, rows), 1)
    ).astype(F32)
    earlier = jnp.dot(below.astype(BF16), named, preferred_element_type=F32)
    places = [
        routes[k] * cap + jnp.sum(earlier * hot[k], axis=1, keepdims=True)
        for k in range(top_count)
    ]

    if lined:
        (
            pick_out,
            pick_in,
            choose,
            weight_in,
            lane_rows,
            lane_scale,
            outgoing,
            arrived,
            scale_out,
            scale_in,
            result,
            returned,
            line_out,
            line_in,
            pick_send,
            pick_recv,
            share_send,
            share_recv,
            lane_send,
            lane_recv,
            disp_send,
            disp_recv,
            back_send,
            back_recv,
            line_send,
            line_recv,
        ) = tail
        plane_slots = n_tp * cap
        slot_lane = lax.broadcasted_iota(jnp.int32, (rows, plane_slots), 1)
        for p in range(n_sp):
            spots = (slot_lane + p * plane_slots).astype(F32)
            for k in range(top_count):
                pick_out[p, k * rows : (k + 1) * rows, :] = (
                    (spots == places[k]).astype(F32).astype(BF16)
                )
        pick_in[seq] = pick_out[seq]
        wide = lax.broadcasted_iota(jnp.int32, (rows, 128), 1)
        shares = jnp.zeros((rows, 128), F32)
        for k in range(top_count):
            shares = jnp.where(wide == k, column(route_weight, k), shares)
        weight_in[seq] = shares

        def pick_copy(target, sender):
            return pltpu.make_async_remote_copy(
                src_ref=pick_out.at[target],
                dst_ref=pick_in.at[sender],
                send_sem=pick_send.at[target],
                recv_sem=pick_recv.at[sender],
                device_id={"sp": target, "tp": ten},
                device_id_type=MESH,
            )

        def share_copy(target, sender):
            return pltpu.make_async_remote_copy(
                src_ref=weight_in.at[sender],
                dst_ref=weight_in.at[sender],
                send_sem=share_send.at[target],
                recv_sem=share_recv.at[sender],
                device_id={"sp": target, "tp": ten},
                device_id_type=MESH,
            )

        for i in range(1, n_sp):
            target = lax.rem(seq + i, n_sp)
            pick_copy(target, seq).start()
            share_copy(target, seq).start()
    else:
        (
            pick_ref,
            outgoing,
            arrived,
            scale_out,
            scale_in,
            result,
            returned,
            disp_send,
            disp_recv,
            back_send,
            back_recv,
        ) = tail
        spots = lax.broadcasted_iota(jnp.int32, (rows, experts * cap), 1).astype(F32)
        for k in range(top_count):
            pick_ref[k * rows : (k + 1) * rows, :] = (
                (spots == places[k]).astype(F32).astype(BF16)
            )

    extra_rows = turned_q_small.shape[1] - size_small

    def fold(size):
        power = 2.0 ** math.floor(math.log2(size**-0.5))
        return power, size**-0.5 / power

    extra_row = lax.broadcasted_iota(jnp.int32, (extra_rows, tokens), 0)
    for kind in range(2):
        heads, size, offset, source, q_ref = (
            (heads_small, size_small, 0, query_small, turned_q_small),
            (heads_large, size_large, heads_small, query_large, turned_q_large),
        )[kind]
        turned = (source[...] * fold(size)[0]).astype(BF16).T
        for h in range(heads):
            chosen = (lax.rem(extra_row, gate_rows) == offset + h) & (extra_row < 3 * gate_rows)
            q_ref[h, :size, :] = turned[h * size : (h + 1) * size, :]
            q_ref[h, size:, :] = jnp.where(chosen, 1.0, 0.0).astype(BF16)
    key_base = (0, piece_small)
    value_base = (piece_small + piece_large, 2 * piece_small + piece_large)

    def attend(block, diagonal):
        block_gates = gates[block]
        if diagonal:
            k_pos = lax.broadcasted_iota(jnp.int32, (tokens, tokens), 0)
            q_pos = lax.broadcasted_iota(jnp.int32, (tokens, tokens), 1)
            seen = q_pos >= k_pos
        for kind in range(2):
            heads, size, piece, offset, q_ref, acc = (
                (heads_small, size_small, piece_small, 0, turned_q_small, acc_small),
                (heads_large, size_large, piece_large, heads_small, turned_q_large, acc_large),
            )[kind]
            kb, vb = key_base[kind], value_base[kind]
            rest = fold(size)[1]
            shift = block_gates * (-1.0 / rest)
            first = shift.astype(BF16).astype(F32)
            second = (shift - first).astype(BF16).astype(F32)
            pieces = [first, second, shift - first - second]
            if extra_rows > 3 * gate_rows:
                pieces.append(jnp.zeros((extra_rows - 3 * gate_rows, tokens), F32))
            keys = jnp.concatenate(
                [kv[block, p, kb : kb + piece, :] for p in range(n_tp)]
                + [jnp.concatenate(pieces, axis=0).astype(BF16)],
                axis=0,
            ).T
            values = jnp.concatenate(
                [kv[block, p, vb : vb + piece, :] for p in range(n_tp)], axis=0
            )
            for h in range(heads):
                g = slice(offset + h, offset + h + 1)
                scores = jnp.dot(keys, q_ref[h], preferred_element_type=F32)
                if diagonal:
                    scores = jnp.where(seen, scores, -jnp.inf)
                block_top = jnp.max(scores, axis=0, keepdims=True)
                top = block_top if diagonal else jnp.maximum(top_ref[g, :], block_top)
                below_top = scores - top
                weights = jnp.exp(below_top if rest == 1.0 else below_top * rest)
                total = jnp.sum(weights, axis=0, keepdims=True)
                mixed = jnp.dot(values, weights.astype(BF16), preferred_element_type=F32)
                if not diagonal:
                    factor = jnp.exp((top_ref[g, :] - top) * rest)
                    total = total_ref[g, :] * factor + total
                    mixed = acc[h] * factor + mixed
                top_ref[g, :] = top
                total_ref[g, :] = total
                acc[h] = mixed

    def pass_on(block):
        kv_copy(block, seq, block).wait_recv()
        for_mates(lambda peer: fwd_copy(block, ten, peer).start())

    attend(seq, True)

    @pl.when(seq > 0)
    def _():
        pass_on(seq - 1)

    def earlier_block(i, carry):
        block = seq - 1 - i

        @pl.when(block > 0)
        def _():
            pass_on(block - 1)

        for_mates(lambda peer: fwd_copy(block, peer, peer).wait_recv())
        gate_copy(block, seq, block).wait_recv()
        attend(block, False)
        return carry

    lax.fori_loop(0, seq, earlier_block, 0)

    for h in range(heads_small):
        attn_t[h * size_small : (h + 1) * size_small, :] = (
            acc_small[h] * (1.0 / total_ref[h : h + 1, :])
        ).astype(BF16)
    for h in range(heads_large):
        first = width_small + h * size_large
        g = heads_small + h
        attn_t[first : first + size_large, :] = (
            acc_large[h] * (1.0 / total_ref[g : g + 1, :])
        ).astype(BF16)
    attn[...] = attn_t[...].T

    def row_ds(group, par):
        return pl.ds(pl.multiple_of((2 * group + par) * rows, rows), rows)

    def pair_copy(c):
        return pltpu.make_async_remote_copy(
            src_ref=pair_out.at[c],
            dst_ref=pair_in.at[c],
            send_sem=pair_send.at[c],
            recv_sem=pair_recv.at[c],
            device_id={"sp": seq, "tp": partner},
            device_id_type=MESH,
        )

    def cross_copy(c, group, source, slot):
        return pltpu.make_async_remote_copy(
            src_ref=cross_out.at[c, group],
            dst_ref=cross_in.at[c, source],
            send_sem=cross_send.at[c, slot],
            recv_sem=cross_recv.at[c, source],
            device_id={"sp": seq, "tp": 2 * group + parity},
            device_id_type=MESH,
        )

    my_group = lax.div(ten, 2)
    for load in loads[:2]:
        load.wait()
    for c in range(cols):
        part = jnp.dot(
            attn[...], proj_w[:, c * col_len : (c + 1) * col_len], preferred_element_type=F32
        )
        proj_f32[c] = part
        for group in range(half_groups):
            pair_out[c, group] = proj_f32[c, row_ds(group, 1 - parity), :].astype(BF16)
        pair_copy(c).start()
    for c in range(cols):
        pair_copy(c).wait_recv()
        for hop in range(1, half_groups):
            group = lax.rem(my_group + hop, half_groups)
            cross_out[c, group] = (
                proj_f32[c, row_ds(group, parity), :] + pair_in[c, group].astype(F32)
            ).astype(BF16)
            cross_copy(c, group, my_group, hop).start()
    def own_rows(c, span, squares):
        value = proj_f32[c, row_ds(my_group, parity), :] + pair_in[c, my_group].astype(F32)
        for hop in range(1, half_groups):
            source = lax.rem(my_group + hop, half_groups)
            cross_copy(c, source, source, hop).wait_recv()
            value = value + cross_in[c, source].astype(F32)
        value = value + residual_in[:, span].astype(F32)
        resid_ref[:, span] = value
        squares = squares + jnp.sum(value * value, axis=1, keepdims=True)
        return value, squares

    def scale_parts(squares):
        scale = lax.rsqrt(squares * (1.0 / width) + 1e-06)
        first = scale.astype(BF16).astype(F32)
        second = (scale - first).astype(BF16).astype(F32)
        third = scale - first - second
        lane = lax.broadcasted_iota(jnp.int32, (rows, 128), 1)
        parts = jnp.where(lane == 0, first, 0.0)
        parts = jnp.where(lane == 1, second, parts)
        return jnp.where(lane == 2, third, parts).astype(BF16)

    if lined:

        def slot_ds(member):
            return pl.ds(pl.multiple_of(member * cap, cap), cap)

        def lane_copy(z, c, up):
            ref = lane_rows.at[z, c] if c < cols else lane_scale.at[z]
            return pltpu.make_async_remote_copy(
                src_ref=ref,
                dst_ref=ref,
                send_sem=lane_send.at[up, z, c],
                recv_sem=lane_recv.at[z, c],
                device_id={"sp": seq + 2 * up - 1, "tp": ten},
                device_id_type=MESH,
            )

        def disp_copy(z, c, peer, sender):
            source, target = (
                (outgoing.at[z, c], arrived.at[z, c])
                if c < cols
                else (scale_out.at[z], scale_in.at[z])
            )
            return pltpu.make_async_remote_copy(
                src_ref=source.at[slot_ds(peer)],
                dst_ref=target.at[slot_ds(sender)],
                send_sem=disp_send.at[z, c, peer],
                recv_sem=disp_recv.at[z, c, sender],
                device_id={"sp": seq, "tp": peer},
                device_id_type=MESH,
            )

        def back_copy(z, c, peer, sender):
            return pltpu.make_async_remote_copy(
                src_ref=result.at[z, c, slot_ds(peer)],
                dst_ref=returned.at[z, c, slot_ds(sender)],
                send_sem=back_send.at[z, c, peer],
                recv_sem=back_recv.at[z, c, sender],
                device_id={"sp": seq, "tp": peer},
                device_id_type=MESH,
            )

        def line_copy(z, c, up):
            return pltpu.make_async_remote_copy(
                src_ref=line_out.at[z, c],
                dst_ref=line_in.at[z + up, c],
                send_sem=line_send.at[z, c],
                recv_sem=line_recv.at[z + up, c],
                device_id={"sp": seq + 2 * up - 1, "tp": ten},
                device_id_type=MESH,
            )

        def go_on(z, c, up):
            if up:

                @pl.when(seq + 1 < n_sp)
                def _():
                    lane_copy(z, c, 1).start()
            else:

                @pl.when(seq > 0)
                def _():
                    lane_copy(z, c, 0).start()

        def place_rows(z, c):
            values = lane_rows[z, c] if c < cols else lane_scale[z]
            placed = jnp.dot(choose[z], values, preferred_element_type=F32).astype(BF16)
            if c < cols:
                outgoing[z, c] = placed
            else:
                scale_out[z] = placed
            for_mates(lambda peer: disp_copy(z, c, peer, ten).start())
            if c < cols:
                arrived[z, c, slot_ds(ten), :] = outgoing[z, c, slot_ds(ten), :]
            else:
                scale_in[z, slot_ds(ten), :] = scale_out[z, slot_ds(ten), :]

        def at_sides(distance, action):
            for up in range(2):
                z = seq - distance if up else seq + distance

                @pl.when(z >= 0 if up else z < n_sp)
                def _():
                    action(z, up)

        def turn_choice(z):
            both = pick_in[z, :rows, :].astype(F32)
            for k in range(1, top_count):
                both = both + pick_in[z, k * rows : (k + 1) * rows, :].astype(F32)
            choose[z] = both.T.astype(BF16)

        def take(distance, c):
            def one(z, up):
                lane_copy(z, c, up).wait_recv()
                go_on(z, c, up)

            def two(z, up):
                if c == 0:
                    pick_copy(seq, z).wait_recv()
                    turn_choice(z)
                place_rows(z, c)

            at_sides(distance, one)
            at_sides(distance, two)

        def serve(z):
            gate_part = jnp.zeros((plane_slots, gate_w.shape[1]), F32)
            up_part = jnp.zeros((plane_slots, gate_w.shape[1]), F32)
            for c in range(cols):
                for_mates(lambda peer: disp_copy(z, c, ten, peer).wait_recv())
                came = arrived[z, c]
                depth = slice(c * col_len, (c + 1) * col_len)
                gate_part = gate_part + jnp.dot(came, gate_w[depth, :], preferred_element_type=F32)
                up_part = up_part + jnp.dot(came, up_w[depth, :], preferred_element_type=F32)
            for_mates(lambda peer: disp_copy(z, cols, ten, peer).wait_recv())
            row_scale = jnp.sum(scale_in[z].astype(F32), axis=1, keepdims=True)
            gate_part, up_part = gate_part * row_scale, up_part * row_scale
            hidden = (gate_part / (1.0 + jnp.exp(-gate_part)) * up_part).astype(BF16)
            for c in range(cols):
                result[z, c] = jnp.dot(
                    hidden, down_w[:, c * col_len : (c + 1) * col_len], preferred_element_type=F32
                ).astype(BF16)
                for_mates(lambda peer: back_copy(z, c, peer, ten).start())
                returned[z, c, slot_ds(ten), :] = result[z, c, slot_ds(ten), :]

        def mixed(z, c):
            for_mates(lambda peer: back_copy(z, c, ten, peer).wait_recv())
            picked = jnp.dot(pick_in[z], returned[z, c], preferred_element_type=F32)
            shares = weight_in[z]
            value = picked[:rows] * shares[:, 0:1]
            for k in range(1, top_count):
                value = value + picked[k * rows : (k + 1) * rows] * shares[:, k : k + 1]
            return value

        def give_back(z, up):
            share_copy(seq, z).wait_recv()
            slot = z + up
            outer = seq > 0 if up else seq + 1 < n_sp
            for c in range(cols):
                value = mixed(z, c)

                @pl.when(outer)
                def _():
                    line_copy(z, c, up).wait_recv()
                    line_out[z, c] = (value + line_in[slot, c].astype(F32)).astype(BF16)

                @pl.when(jnp.logical_not(outer))
                def _():
                    line_out[z, c] = value.astype(BF16)

                line_copy(z, c, up).start()

        def chain(j):
            @pl.when(n_sp - 1 - j < seq)
            def _():
                give_back(n_sp - 1 - j, 0)

            @pl.when(j > seq)
            def _():
                give_back(j, 1)

        turn_choice(seq)
        squares = jnp.zeros((rows, 1), F32)
        gain = norm_gain[...].astype(F32).reshape(1, width)
        for c in range(cols):
            span = slice(c * col_len, (c + 1) * col_len)
            value, squares = own_rows(c, span, squares)
            lane_rows[seq, c] = (value * gain[:, span]).astype(BF16)
            go_on(seq, c, 0)
            go_on(seq, c, 1)
            place_rows(seq, c)
        lane_scale[seq] = scale_parts(squares)
        go_on(seq, cols, 0)
        go_on(seq, cols, 1)
        place_rows(seq, cols)
        for load in loads[2:]:
            load.wait()

        for step in range(1, n_sp + 2):
            moving = step < n_sp
            if moving:
                take(step, 0)
            if step == 2:
                for c in range(cols):
                    span = slice(c * col_len, (c + 1) * col_len)
                    resid_ref[:, span] = resid_ref[:, span] + mixed(seq, c)
            elif step > 2:
                chain(step - 2)
            if moving:
                take(step, 1)
            if step == 1:
                for c in range(2, cols + 1):
                    take(step, c)
                serve(seq)
            elif step <= n_sp:
                at_sides(step - 1, lambda z, up: serve(z))
                if moving:
                    for c in range(2, cols + 1):
                        take(step, c)

        for c in range(cols):
            span = slice(c * col_len, (c + 1) * col_len)
            for up in range(2):

                @pl.when(seq > 0 if up else seq + 1 < n_sp)
                def _():
                    line_copy(seq, c, up).wait_recv()
                    resid_ref[:, span] = resid_ref[:, span] + line_in[seq + up, c].astype(F32)

            out[:, span] = resid_ref[:, span].astype(BF16)

        for i in range(1, n_sp):
            target = lax.rem(seq + i, n_sp)
            pick_copy(target, seq).wait_send()
            share_copy(target, seq).wait_send()

        def sent_lane(z, c, up):
            @pl.when(seq + 1 < n_sp if up else seq > 0)
            def _():
                lane_copy(z, c, up).wait_send()

        def sent_block(z, carry):
            for c in range(cols + 1):
                for_mates(lambda peer: disp_copy(z, c, peer, ten).wait_send())
                if c < cols:
                    for_mates(lambda peer: back_copy(z, c, peer, ten).wait_send())
                for up in range(2):

                    @pl.when(z <= seq if up else z >= seq)
                    def _():
                        sent_lane(z, c, up)

                if c < cols:

                    @pl.when(z < seq)
                    def _():
                        line_copy(z, c, 0).wait_send()

                    @pl.when(z > seq)
                    def _():
                        line_copy(z, c, 1).wait_send()

            return carry

        lax.fori_loop(0, n_sp, sent_block, 0)
    else:
        def slot_ds(peer):
            return pl.ds(pl.multiple_of(peer * cap, cap), cap)

        def exchange(source_ref, target_ref, send, recv, peer, sender):
            return pltpu.make_async_remote_copy(
                src_ref=source_ref.at[slot_ds(peer)],
                dst_ref=target_ref.at[slot_ds(sender)],
                send_sem=send.at[peer],
                recv_sem=recv.at[sender],
                device_id={"sp": lax.div(peer, n_tp), "tp": lax.rem(peer, n_tp)},
                device_id_type=MESH,
            )

        def part_copy(c, peer, sender):
            if c < cols:
                source_ref, target_ref = outgoing.at[c], arrived.at[c]
            else:
                source_ref, target_ref = scale_out, scale_in
            return exchange(source_ref, target_ref, disp_send.at[c], disp_recv.at[c], peer, sender)

        def for_members(plane, action):
            def one(j, carry):
                peer = plane * n_tp + lax.rem(ten + j, n_tp)

                @pl.when(peer != me)
                def _():
                    action(peer)

                return carry

            lax.fori_loop(0, n_tp, one, 0)

        slots = experts * cap
        block_rows = min(256, slots)

        def place_rows(values, c):
            for b in range(slots // block_rows):
                span = slice(b * block_rows, (b + 1) * block_rows)
                chosen = pick_ref[:rows, span]
                for k in range(1, top_count):
                    chosen = chosen + pick_ref[k * rows : (k + 1) * rows, span]
                placed = lax.dot_general(
                    chosen, values, (((0,), (0,)), ((), ())), preferred_element_type=F32
                ).astype(BF16)
                if c < cols:
                    outgoing[c, span, :] = placed
                else:
                    scale_out[span, :] = placed

            def dispatch(i, carry):
                for_members(
                    lax.rem(seq + n_sp - i, n_sp), lambda peer: part_copy(c, peer, me).start()
                )
                return carry

            lax.fori_loop(0, n_sp, dispatch, 0)

        squares = jnp.zeros((rows, 1), F32)
        gain = norm_gain[...].astype(F32).reshape(1, width)
        for c in range(cols):
            span = slice(c * col_len, (c + 1) * col_len)
            value, squares = own_rows(c, span, squares)
            place_rows((value * gain[:, span]).astype(BF16), c)
        place_rows(scale_parts(squares), cols)
        for c in range(cols):
            arrived[c, slot_ds(me), :] = outgoing[c, slot_ds(me), :]
        scale_in[slot_ds(me), :] = scale_out[slot_ds(me), :]
        for load in loads[2:]:
            load.wait()

        group_rows = n_tp * cap

        def serve(i, carry):
            plane = lax.rem(seq + i, n_sp)
            span = pl.ds(pl.multiple_of(plane * group_rows, group_rows), group_rows)
            gate_part = jnp.zeros((group_rows, gate_w.shape[1]), F32)
            up_part = jnp.zeros((group_rows, gate_w.shape[1]), F32)
            for c in range(cols):
                for_members(plane, lambda peer: part_copy(c, me, peer).wait_recv())
                came = arrived[c, span, :]
                depth = slice(c * col_len, (c + 1) * col_len)
                gate_part = gate_part + jnp.dot(came, gate_w[depth, :], preferred_element_type=F32)
                up_part = up_part + jnp.dot(came, up_w[depth, :], preferred_element_type=F32)
            for_members(plane, lambda peer: part_copy(cols, me, peer).wait_recv())
            row_scale = jnp.sum(scale_in[span, :].astype(F32), axis=1, keepdims=True)
            gate_part, up_part = gate_part * row_scale, up_part * row_scale
            hidden = (gate_part / (1.0 + jnp.exp(-gate_part)) * up_part).astype(BF16)
            result[span, :] = jnp.dot(hidden, down_w[...], preferred_element_type=F32).astype(BF16)
            for_members(
                plane,
                lambda peer: exchange(result, returned, back_send, back_recv, peer, me).start(),
            )
            return carry

        lax.fori_loop(0, n_sp, serve, 0)
        returned[slot_ds(me), :] = result[slot_ds(me), :]

        def collect(i, carry):
            peer = lax.rem(me + i, experts)
            exchange(result, returned, back_send, back_recv, me, peer).wait_recv()
            return carry

        lax.fori_loop(1, experts, collect, 0)
        for c in range(cols):
            span = slice(c * col_len, (c + 1) * col_len)
            picked = jnp.dot(pick_ref[...], returned[:, span], preferred_element_type=F32)
            value = resid_ref[:, span]
            for k in range(top_count):
                value = value + picked[k * rows : (k + 1) * rows] * column(route_weight, k)
            out[:, span] = value.astype(BF16)

        def sent_rows(i, carry):
            peer = lax.rem(me + i, experts)
            for c in range(cols + 1):
                part_copy(c, peer, me).wait_send()
            exchange(result, returned, back_send, back_recv, peer, me).wait_send()
            return carry

        lax.fori_loop(1, experts, sent_rows, 0)

    def sent_kv(target, carry):
        gate_copy(seq, target, target).wait_send()
        kv_copy(seq, target, target).wait_send()
        return carry

    lax.fori_loop(seq + 1, n_sp, sent_kv, 0)

    def sent_fwd(block, carry):
        for_mates(lambda peer: fwd_copy(block, ten, peer).wait_send())
        return carry

    lax.fori_loop(0, seq, sent_fwd, 0)
    for c in range(cols):
        pair_copy(c).wait_send()
        for hop in range(1, half_groups):
            group = lax.rem(my_group + hop, half_groups)
            cross_copy(c, group, my_group, hop).wait_send()


def shards(
    residual_in,
    query_small,
    query_large,
    key_small,
    key_large,
    value_small,
    value_large,
    forget_small,
    forget_large,
    project_small,
    project_large,
    norm_gain,
    expert_gate,
    expert_up,
    expert_down,
    routing,
    route_weight,
):
    n_sp, n_tp = lax.axis_size("sp"), lax.axis_size("tp")
    experts = n_sp * n_tp
    rows, width = residual_in.shape
    top_count = routing.shape[1]
    tokens = query_small.shape[0]
    size_small, size_large = key_small.shape[0], key_large.shape[0]
    heads_small, heads_large = forget_small.shape[0], forget_large.shape[0]
    heads = heads_small + heads_large
    gate_rows = -(-heads // 8) * 8
    extra_rows = -(-3 * gate_rows // 16) * 16
    capacity = max(2, 2 * rows * top_count // experts)
    cap = -(-capacity // 16) * 16
    col_len = min(width, 512)
    cols = width // col_len
    hidden = expert_gate.shape[2]
    attn_width = heads_small * size_small + heads_large * size_large
    half_groups = n_tp // 2
    slots = experts * cap
    group = n_tp * cap
    lined = n_tp * capacity >= rows
    vmem, dma = pltpu.VMEM, pltpu.SemaphoreType.DMA
    if lined:
        tail = [
            vmem((n_sp, top_count * rows, group), BF16),
            vmem((n_sp, top_count * rows, group), BF16),
            vmem((n_sp, group, rows), BF16),
            vmem((n_sp, rows, 128), F32),
            vmem((n_sp, cols, rows, col_len), BF16),
            vmem((n_sp, rows, 128), BF16),
            vmem((n_sp, cols, group, col_len), BF16),
            vmem((n_sp, cols, group, col_len), BF16),
            vmem((n_sp, group, 128), BF16),
            vmem((n_sp, group, 128), BF16),
            vmem((n_sp, cols, group, col_len), BF16),
            vmem((n_sp, cols, group, col_len), BF16),
            vmem((n_sp, cols, rows, col_len), BF16),
            vmem((n_sp + 1, cols, rows, col_len), BF16),
            dma((n_sp,)),
            dma((n_sp,)),
            dma((n_sp,)),
            dma((n_sp,)),
            dma((2, n_sp, cols + 1)),
            dma((n_sp, cols + 1)),
            dma((n_sp, cols + 1, n_tp)),
            dma((n_sp, cols + 1, n_tp)),
            dma((n_sp, cols, n_tp)),
            dma((n_sp, cols, n_tp)),
            dma((n_sp, cols)),
            dma((n_sp + 1, cols)),
        ]
    else:
        tail = [
            vmem((top_count * rows, slots), BF16),
            vmem((cols, slots, col_len), BF16),
            vmem((cols, slots, col_len), BF16),
            vmem((slots, 128), BF16),
            vmem((slots, 128), BF16),
            vmem((slots, width), BF16),
            vmem((slots, width), BF16),
            dma((cols + 1, experts)),
            dma((cols + 1, experts)),
            dma((experts,)),
            dma((experts,)),
        ]
    return pl.pallas_call(
        functools.partial(layer_kernel, (n_sp, n_tp, cap, col_len, lined)),
        out_shape=jax.ShapeDtypeStruct((rows, width), BF16),
        in_specs=[pl.BlockSpec(memory_space=pltpu.VMEM)] * 12
        + [pl.BlockSpec(memory_space=pl.ANY)] * 5,
        out_specs=pl.BlockSpec(memory_space=pltpu.VMEM),
        scratch_shapes=[
            vmem((n_sp, n_tp, 2 * (size_small + size_large) // n_tp, tokens), BF16),
            vmem((n_sp, gate_rows, tokens), F32),
            vmem((heads_small, size_small + extra_rows, tokens), BF16),
            vmem((heads_large, size_large + extra_rows, tokens), BF16),
            vmem((gate_rows, tokens), F32),
            vmem((gate_rows, tokens), F32),
            vmem((heads_small, size_small, tokens), F32),
            vmem((heads_large, size_large, tokens), F32),
            vmem((attn_width, tokens), BF16),
            vmem((tokens, attn_width), BF16),
            vmem((attn_width, width), BF16),
            vmem((width, hidden), BF16),
            vmem((width, hidden), BF16),
            vmem((hidden, width), BF16),
            vmem((cols, tokens, col_len), F32),
            vmem((cols, half_groups, rows, col_len), BF16),
            vmem((cols, half_groups, rows, col_len), BF16),
            vmem((cols, half_groups, rows, col_len), BF16),
            vmem((cols, half_groups, rows, col_len), BF16),
            vmem((rows, width), F32),
            dma((5,)),
            dma((n_sp,)),
            dma((n_sp,)),
            dma((n_sp,)),
            dma((n_sp,)),
            dma((n_sp, n_tp)),
            dma((n_sp, n_tp)),
            dma((cols,)),
            dma((cols,)),
            dma((cols, half_groups)),
            dma((cols, half_groups)),
        ]
        + tail,
        compiler_params=pltpu.CompilerParams(
            collective_id=0, has_side_effects=True, vmem_limit_bytes=60 * 1024 * 1024
        ),
    )(
        residual_in,
        query_small,
        query_large,
        key_small,
        key_large,
        value_small,
        value_large,
        forget_small,
        forget_large,
        norm_gain,
        routing.T,
        route_weight.T,
        project_small,
        project_large,
        expert_gate,
        expert_up,
        expert_down,
    )


def solution(mesh):
    in_specs = (
        P(("grp", "sp", "tp"), None),
        P(("grp", "sp"), "tp"),
        P(("grp", "sp"), "tp"),
        P(None, ("grp", "sp")),
        P(None, ("grp", "sp")),
        P(None, ("grp", "sp")),
        P(None, ("grp", "sp")),
        P("tp", ("grp", "sp")),
        P("tp", ("grp", "sp")),
        P("tp", None),
        P("tp", None),
        P(),
        P(("sp", "tp"), None, None),
        P(("sp", "tp"), None, None),
        P(("sp", "tp"), None, None),
        P(("grp", "sp", "tp"), None),
        P(("grp", "sp", "tp"), None),
    )
    out_specs = P(("grp", "sp", "tp"), None)
    return jax.shard_map(shards, mesh=mesh, in_specs=in_specs, out_specs=out_specs, check_vma=False)
```

time: 81.3 us -> 86.6 us (1.065)
  the two profiles are of different devices: /device:TPU:13 before, /device:TPU:24 now
where the time goes in v2:
time: 86.6 us; the launch traced here: 86.5 us
  Pallas kernels  84.8 us (98%)
  local copies, waits for them, and re-layouts  1.67 us (2%)
    pallas_call x1, Pallas kernels, shards(): pl.pallas_call(functools.partial(layer_kernel, (n_sp, n_tp, cap, col_len,...  84.8 us

profile of v2, /device:TPU:24, one launch (start us, length us, event | category | flops | bytes accessed | tf_op | source)
XLA Modules:
  0.0 86.5 jit_solution(1631733412260618201)
XLA Ops:
  0.0 84.8 %shard_map.163 = bf16[64,2048]{1,0:T(8,128)(2,1)} custom-call(bf16[64,2048]{1,0:T(8,128)(2,1)} %refs_0_.1, bf16[256,256]{1,0:T(8,128)(2,1)} %refs_1_.1, bf16[256,256]{1,0:T(8,128)(2,1)} %refs_2_.1, bf16[64,256]{1,0:T(8,128)(2,1)} %refs_3_.1, bf16[128,256]{1,0:T(8,128)(2,1)} %refs_4_.1, bf16[64,256]{1,0:T(8,128)(2,1)} %refs_5_.1, bf16[128,256]{1,0:T(8,128)(2,1)} %refs_6_.1, ...), custom_call_target="tpu_custom_call" | custom-call | tf_op jit(solution)/shard_map/pallas_call | solution.py:925
  84.8 1.7 %copy.19 = bf16[64,2048]{1,0:T(8,128)(2,1)} copy(bf16[64,2048]{1,0:T(8,128)(2,1)} %shard_map.163) | data formatting | bytes 524288

commit v3 on v2

--- a/solution.py
+++ b/solution.py
@@ -58,8 +58,9 @@
         kv_recv,
         gate_send,
         gate_recv,
-        fwd_send,
-        fwd_recv,
+        share_send,
+        side_recv,
+        pass_recv,
         pair_send,
         pair_recv,
         cross_send,
@@ -81,6 +82,7 @@
     piece_small, piece_large = size_small // n_tp, size_large // n_tp
     cols = width // col_len
     half_groups = n_tp // 2
+    my_group = lax.div(ten, 2)
 
     loads = [
         pltpu.make_async_copy(project_small, proj_w.at[pl.ds(0, width_small)], weight_sem.at[0]),
@@ -93,9 +95,6 @@
         pltpu.make_async_copy(expert_up.at[0], up_w, weight_sem.at[3]),
         pltpu.make_async_copy(expert_down.at[0], down_w, weight_sem.at[4]),
     ]
-    for load in loads:
-        load.start()
-
     barrier = pltpu.get_barrier_semaphore()
 
     def greet(peer_sp, peer_tp):
@@ -103,19 +102,12 @@
             barrier, inc=1, device_id={"sp": peer_sp, "tp": peer_tp}, device_id_type=MESH
         )
 
-    if lined:
-        for i in range(1, n_tp):
-            greet(seq, lax.rem(ten + i, n_tp))
-        for i in range(1, n_sp):
-            greet(lax.rem(seq + i, n_sp), ten)
-    else:
-
-        def greet_all(i, carry):
-            peer = lax.rem(me + i, experts)
-            greet(lax.div(peer, n_tp), lax.rem(peer, n_tp))
-            return carry
-
-        lax.fori_loop(1, experts, greet_all, 0)
+    def greet_all(i, carry):
+        peer = lax.rem(me + i, experts)
+        greet(lax.div(peer, n_tp), lax.rem(peer, n_tp))
+        return carry
+
+    lax.fori_loop(1, experts, greet_all, 0)
 
     for p in range(n_tp):
         base = 0
@@ -127,15 +119,14 @@
         ):
             kv[seq, p, base : base + piece, :] = source[p * piece : (p + 1) * piece, :]
             base += piece
-    gates[seq, :heads_small, :] = forget_small[...]
-    gates[seq, heads_small : heads_small + heads_large, :] = forget_large[...]
+    top_count = routing.shape[0]
     gate_rows = gates.shape[1]
-    if gate_rows > heads_small + heads_large:
-        gates[seq, heads_small + heads_large :, :] = jnp.zeros(
-            (gate_rows - heads_small - heads_large, tokens), F32
-        )
-
-    pl.semaphore_wait(barrier, n_tp + n_sp - 2 if lined else experts - 1)
+    gates[seq] = jnp.zeros(gates.shape[1:], F32)
+    gates[seq, :heads_small, :tokens] = forget_small[...]
+    gates[seq, heads_small : heads_small + heads_large, :tokens] = forget_large[...]
+    gates[seq, :top_count, tokens : tokens + rows] = routing[...].astype(F32)
+
+    pl.semaphore_wait(barrier, experts - 1)
 
     def kv_copy(source, target, slot):
         return pltpu.make_async_remote_copy(
@@ -157,13 +148,27 @@
             device_id_type=MESH,
         )
 
-    def fwd_copy(source, piece, peer):
+    def other_group(hop):
+        return lax.rem(my_group + hop, half_groups)
+
+    def side_copy(source, group_from, group_to):
+        piece = kv.at[source, 2 * group_from + parity]
+        return pltpu.make_async_remote_copy(
+            src_ref=piece,
+            dst_ref=piece,
+            send_sem=share_send.at[source],
+            recv_sem=side_recv.at[source, group_from],
+            device_id={"sp": seq, "tp": 2 * group_to + parity},
+            device_id_type=MESH,
+        )
+
+    def pass_copy(source, piece):
         return pltpu.make_async_remote_copy(
             src_ref=kv.at[source, piece],
             dst_ref=kv.at[source, piece],
-            send_sem=fwd_send.at[source, peer],
-            recv_sem=fwd_recv.at[source, piece],
-            device_id={"sp": seq, "tp": peer},
+            send_sem=share_send.at[source],
+            recv_sem=pass_recv.at[source],
+            device_id={"sp": seq, "tp": partner},
             device_id_type=MESH,
         )
 
@@ -176,7 +181,15 @@
         kv_copy(seq, target, target).start()
         return carry
 
+    def send_gates(target, carry):
+        gate_copy(seq, target, target).start()
+        return carry
+
     lax.fori_loop(seq + 1, n_sp, send_kv, 0)
+    if lined:
+        lax.fori_loop(0, seq, send_gates, 0)
+    for load in loads:
+        load.start()
 
     lanes = lax.broadcasted_iota(jnp.int32, (rows, experts), 1)
     same = lax.broadcasted_iota(jnp.int32, (rows, rows), 0) == lax.broadcasted_iota(
@@ -188,26 +201,23 @@
             jnp.where(same, ref[k : k + 1, :].astype(F32), 0.0), axis=1, keepdims=True
         )
 
-    top_count = routing.shape[0]
-    routes = [column(routing, k) for k in range(top_count)]
-    hot = [(routes[k] == lanes.astype(F32)).astype(F32) for k in range(top_count)]
-    named = sum(hot).astype(BF16)
-    below = (
-        lax.broadcasted_iota(jnp.int32, (rows, rows), 0)
-        > lax.broadcasted_iota(jnp.int32, (rows, rows), 1)
-    ).astype(F32)
-    earlier = jnp.dot(below.astype(BF16), named, preferred_element_type=F32)
-    places = [
-        routes[k] * cap + jnp.sum(earlier * hot[k], axis=1, keepdims=True)
-        for k in range(top_count)
-    ]
+    def route_places(routes):
+        hot = [(route == lanes.astype(F32)).astype(F32) for route in routes]
+        named = sum(hot).astype(BF16)
+        below = (
+            lax.broadcasted_iota(jnp.int32, (rows, rows), 0)
+            > lax.broadcasted_iota(jnp.int32, (rows, rows), 1)
+        ).astype(F32)
+        earlier = jnp.dot(below.astype(BF16), named, preferred_element_type=F32)
+        return [
+            route * cap + jnp.sum(earlier * one, axis=1, keepdims=True)
+            for route, one in zip(routes, hot)
+        ]
 
     if lined:
         (
-            pick_out,
-            pick_in,
+            pick_ref,
             choose,
-            weight_in,
             lane_rows,
             lane_scale,
             outgoing,
@@ -216,60 +226,25 @@
             scale_in,
             result,
             returned,
-            line_out,
-            line_in,
-            pick_send,
-            pick_recv,
-            share_send,
-            share_recv,
             lane_send,
             lane_recv,
             disp_send,
             disp_recv,
             back_send,
             back_recv,
-            line_send,
-            line_recv,
         ) = tail
         plane_slots = n_tp * cap
         slot_lane = lax.broadcasted_iota(jnp.int32, (rows, plane_slots), 1)
-        for p in range(n_sp):
-            spots = (slot_lane + p * plane_slots).astype(F32)
-            for k in range(top_count):
-                pick_out[p, k * rows : (k + 1) * rows, :] = (
-                    (spots == places[k]).astype(F32).astype(BF16)
-                )
-        pick_in[seq] = pick_out[seq]
-        wide = lax.broadcasted_iota(jnp.int32, (rows, 128), 1)
-        shares = jnp.zeros((rows, 128), F32)
-        for k in range(top_count):
-            shares = jnp.where(wide == k, column(route_weight, k), shares)
-        weight_in[seq] = shares
-
-        def pick_copy(target, sender):
-            return pltpu.make_async_remote_copy(
-                src_ref=pick_out.at[target],
-                dst_ref=pick_in.at[sender],
-                send_sem=pick_send.at[target],
-                recv_sem=pick_recv.at[sender],
-                device_id={"sp": target, "tp": ten},
-                device_id_type=MESH,
-            )
-
-        def share_copy(target, sender):
-            return pltpu.make_async_remote_copy(
-                src_ref=weight_in.at[sender],
-                dst_ref=weight_in.at[sender],
-                send_sem=share_send.at[target],
-                recv_sem=share_recv.at[sender],
-                device_id={"sp": target, "tp": ten},
-                device_id_type=MESH,
-            )
-
-        for i in range(1, n_sp):
-            target = lax.rem(seq + i, n_sp)
-            pick_copy(target, seq).start()
-            share_copy(target, seq).start()
+
+        def prepare(z):
+            known = gates[z][:, tokens : tokens + rows]
+            spots = (slot_lane + seq * plane_slots).astype(F32)
+            both = jnp.zeros((rows, plane_slots), F32)
+            for place in route_places([column(known, k) for k in range(top_count)]):
+                both = both + (spots == place).astype(F32)
+            choose[z] = both.T.astype(BF16)
+
+        prepare(seq)
     else:
         (
             pick_ref,
@@ -284,11 +259,11 @@
             back_send,
             back_recv,
         ) = tail
-        spots = lax.broadcasted_iota(jnp.int32, (rows, experts * cap), 1).astype(F32)
-        for k in range(top_count):
-            pick_ref[k * rows : (k + 1) * rows, :] = (
-                (spots == places[k]).astype(F32).astype(BF16)
-            )
+
+    spots = lax.broadcasted_iota(jnp.int32, (rows, experts * cap), 1).astype(F32)
+    places = route_places([column(routing, k) for k in range(top_count)])
+    for k in range(top_count):
+        pick_ref[k * rows : (k + 1) * rows, :] = (spots == places[k]).astype(F32).astype(BF16)
 
     extra_rows = turned_q_small.shape[1] - size_small
 
@@ -311,7 +286,7 @@
     value_base = (piece_small + piece_large, 2 * piece_small + piece_large)
 
     def attend(block, diagonal):
-        block_gates = gates[block]
+        block_gates = gates[block][:, :tokens]
         if diagonal:
             k_pos = lax.broadcasted_iota(jnp.int32, (tokens, tokens), 0)
             q_pos = lax.broadcasted_iota(jnp.int32, (tokens, tokens), 1)
@@ -356,29 +331,50 @@
                 total_ref[g, :] = total
                 acc[h] = mixed
 
-    def pass_on(block):
+    def share_out(block):
         kv_copy(block, seq, block).wait_recv()
-        for_mates(lambda peer: fwd_copy(block, ten, peer).start())
+        for hop in range(1, half_groups):
+            side_copy(block, my_group, other_group(hop)).start()
+        pass_copy(block, ten).start()
+
+    def hand_on(block):
+        for hop in range(1, half_groups):
+            group = other_group(hop)
+            side_copy(block, group, group).wait_recv()
+            pass_copy(block, 2 * group + parity).start()
 
     attend(seq, True)
 
     @pl.when(seq > 0)
     def _():
-        pass_on(seq - 1)
+        share_out(seq - 1)
+
+    if lined:
+        for i in range(1, n_sp):
+            z = lax.rem(seq + i, n_sp)
+            gate_copy(z, seq, z).wait_recv()
+            prepare(z)
 
     def earlier_block(i, carry):
-        block = seq - 1 - i
-
-        @pl.when(block > 0)
+        @pl.when(i < seq)
         def _():
-            pass_on(block - 1)
-
-        for_mates(lambda peer: fwd_copy(block, peer, peer).wait_recv())
-        gate_copy(block, seq, block).wait_recv()
-        attend(block, False)
+            share_out(seq - 1 - i)
+
+        @pl.when(i <= seq)
+        def _():
+            hand_on(seq - i)
+
+        @pl.when(i > 1)
+        def _():
+            block = seq + 1 - i
+            pass_copy(block, pl.ds(0, half_groups)).wait_recv()
+            if not lined:
+                gate_copy(block, seq, block).wait_recv()
+            attend(block, False)
+
         return carry
 
-    lax.fori_loop(0, seq, earlier_block, 0)
+    lax.fori_loop(1, jnp.where(seq > 0, seq + 2, 1), earlier_block, 0)
 
     for h in range(heads_small):
         attn_t[h * size_small : (h + 1) * size_small, :] = (
@@ -399,23 +395,22 @@
         return pltpu.make_async_remote_copy(
             src_ref=pair_out.at[c],
             dst_ref=pair_in.at[c],
-            send_sem=pair_send.at[c],
+            send_sem=pair_send.at[0],
             recv_sem=pair_recv.at[c],
             device_id={"sp": seq, "tp": partner},
             device_id_type=MESH,
         )
 
-    def cross_copy(c, group, source, slot):
+    def cross_copy(c, group, source, slot, part=None):
         return pltpu.make_async_remote_copy(
             src_ref=cross_out.at[c, group],
             dst_ref=cross_in.at[c, source],
-            send_sem=cross_send.at[c, slot],
-            recv_sem=cross_recv.at[c, source],
+            send_sem=cross_send.at[slot],
+            recv_sem=cross_recv.at[c if part is None else part, source],
             device_id={"sp": seq, "tp": 2 * group + parity},
             device_id_type=MESH,
         )
 
-    my_group = lax.div(ten, 2)
     for load in loads[:2]:
         load.wait()
     for c in range(cols):
@@ -445,6 +440,15 @@
         squares = squares + jnp.sum(value * value, axis=1, keepdims=True)
         return value, squares
 
+    def finish():
+        for c in range(cols):
+            span = slice(c * col_len, (c + 1) * col_len)
+            picked = jnp.dot(pick_ref[...], returned[:, span], preferred_element_type=F32)
+            value = resid_ref[:, span]
+            for k in range(top_count):
+                value = value + picked[k * rows : (k + 1) * rows] * column(route_weight, k)
+            out[:, span] = value.astype(BF16)
+
     def scale_parts(squares):
         scale = lax.rsqrt(squares * (1.0 / width) + 1e-06)
         first = scale.astype(BF16).astype(F32)
@@ -465,7 +469,7 @@
             return pltpu.make_async_remote_copy(
                 src_ref=ref,
                 dst_ref=ref,
-                send_sem=lane_send.at[up, z, c],
+                send_sem=lane_send.at[up, z, 1 if c == cols else 0],
                 recv_sem=lane_recv.at[z, c],
                 device_id={"sp": seq + 2 * up - 1, "tp": ten},
                 device_id_type=MESH,
@@ -480,31 +484,54 @@
             return pltpu.make_async_remote_copy(
                 src_ref=source.at[slot_ds(peer)],
                 dst_ref=target.at[slot_ds(sender)],
-                send_sem=disp_send.at[z, c, peer],
-                recv_sem=disp_recv.at[z, c, sender],
+                send_sem=disp_send.at[z, 1 if c == cols else 0],
+                recv_sem=disp_recv.at[z, c],
                 device_id={"sp": seq, "tp": peer},
                 device_id_type=MESH,
             )
 
-        def back_copy(z, c, peer, sender):
+        def back_copy(z, peer):
             return pltpu.make_async_remote_copy(
-                src_ref=result.at[z, c, slot_ds(peer)],
-                dst_ref=returned.at[z, c, slot_ds(sender)],
-                send_sem=back_send.at[z, c, peer],
-                recv_sem=back_recv.at[z, c, sender],
-                device_id={"sp": seq, "tp": peer},
+                src_ref=result.at[z, slot_ds(peer)],
+                dst_ref=returned.at[slot_ds(me)],
+                send_sem=back_send.at[0],
+                recv_sem=back_recv.at[0],
+                device_id={"sp": z, "tp": peer},
                 device_id_type=MESH,
             )
 
-        def line_copy(z, c, up):
+        mates_rows = pl.ds(0, (n_tp - 1) * cap)
+        next_mate = lax.rem(ten + 1, n_tp)
+
+        def bulk(source, target, send_sem, recv_sem):
             return pltpu.make_async_remote_copy(
-                src_ref=line_out.at[z, c],
-                dst_ref=line_in.at[z + up, c],
-                send_sem=line_send.at[z, c],
-                recv_sem=line_recv.at[z + up, c],
-                device_id={"sp": seq + 2 * up - 1, "tp": ten},
+                src_ref=source,
+                dst_ref=target,
+                send_sem=send_sem,
+                recv_sem=recv_sem,
+                device_id={"sp": seq, "tp": next_mate},
                 device_id_type=MESH,
             )
+
+        def disp_came(z, c):
+            ref = arrived.at[z, c, mates_rows] if c < cols else scale_in.at[z, mates_rows]
+            bulk(ref, ref, disp_send.at[z, 0], disp_recv.at[z, c]).wait_recv()
+
+        def sent_plane(z):
+            ref = outgoing.at[z, :, mates_rows]
+            bulk(ref, ref, disp_send.at[z, 0], disp_recv.at[z, 0]).wait_send()
+            ref = scale_out.at[z, mates_rows]
+            bulk(ref, ref, disp_send.at[z, 1], disp_recv.at[z, 0]).wait_send()
+
+        def sent_lane(z, up):
+            @pl.when(seq + 1 < n_sp if up else seq > 0)
+            def _():
+                bulk(
+                    lane_rows.at[z], lane_rows.at[z], lane_send.at[up, z, 0], lane_recv.at[z, 0]
+                ).wait_send()
+                bulk(
+                    lane_scale.at[z], lane_scale.at[z], lane_send.at[up, z, 1], lane_recv.at[z, 0]
+                ).wait_send()
 
         def go_on(z, c, up):
             if up:
@@ -531,91 +558,79 @@
             else:
                 scale_in[z, slot_ds(ten), :] = scale_out[z, slot_ds(ten), :]
 
-        def at_sides(distance, action):
-            for up in range(2):
-                z = seq - distance if up else seq + distance
-
-                @pl.when(z >= 0 if up else z < n_sp)
+        def at_pair(k, action, own):
+            low, high = seq - k - 1, seq + k
+
+            @pl.when(low >= 0)
+            def _():
+                action(low, 1)
+
+            if k > 0:
+
+                @pl.when(high < n_sp)
                 def _():
-                    action(z, up)
-
-        def turn_choice(z):
-            both = pick_in[z, :rows, :].astype(F32)
-            for k in range(1, top_count):
-                both = both + pick_in[z, k * rows : (k + 1) * rows, :].astype(F32)
-            choose[z] = both.T.astype(BF16)
-
-        def take(distance, c):
+                    action(high, 0)
+            elif own is not None:
+                own()
+
+        def take(k, c):
             def one(z, up):
                 lane_copy(z, c, up).wait_recv()
                 go_on(z, c, up)
-
-            def two(z, up):
-                if c == 0:
-                    pick_copy(seq, z).wait_recv()
-                    turn_choice(z)
                 place_rows(z, c)
 
-            at_sides(distance, one)
-            at_sides(distance, two)
-
-        def serve(z):
-            gate_part = jnp.zeros((plane_slots, gate_w.shape[1]), F32)
-            up_part = jnp.zeros((plane_slots, gate_w.shape[1]), F32)
+            at_pair(k, one, None)
+
+        def serve(*blocks):
+            count = len(blocks) * plane_slots
+            gate_part = jnp.zeros((count, gate_w.shape[1]), F32)
+            up_part = jnp.zeros((count, gate_w.shape[1]), F32)
             for c in range(cols):
-                for_mates(lambda peer: disp_copy(z, c, ten, peer).wait_recv())
-                came = arrived[z, c]
+                for z in blocks:
+                    disp_came(z, c)
+                came = jnp.concatenate([arrived[z, c] for z in blocks], axis=0)
                 depth = slice(c * col_len, (c + 1) * col_len)
                 gate_part = gate_part + jnp.dot(came, gate_w[depth, :], preferred_element_type=F32)
                 up_part = up_part + jnp.dot(came, up_w[depth, :], preferred_element_type=F32)
-            for_mates(lambda peer: disp_copy(z, cols, ten, peer).wait_recv())
-            row_scale = jnp.sum(scale_in[z].astype(F32), axis=1, keepdims=True)
+            for z in blocks:
+                disp_came(z, cols)
+            row_scale = jnp.concatenate(
+                [jnp.sum(scale_in[z].astype(F32), axis=1, keepdims=True) for z in blocks], axis=0
+            )
             gate_part, up_part = gate_part * row_scale, up_part * row_scale
             hidden = (gate_part / (1.0 + jnp.exp(-gate_part)) * up_part).astype(BF16)
             for c in range(cols):
-                result[z, c] = jnp.dot(
-                    hidden, down_w[:, c * col_len : (c + 1) * col_len], preferred_element_type=F32
-                ).astype(BF16)
-                for_mates(lambda peer: back_copy(z, c, peer, ten).start())
-                returned[z, c, slot_ds(ten), :] = result[z, c, slot_ds(ten), :]
-
-        def mixed(z, c):
-            for_mates(lambda peer: back_copy(z, c, ten, peer).wait_recv())
-            picked = jnp.dot(pick_in[z], returned[z, c], preferred_element_type=F32)
-            shares = weight_in[z]
-            value = picked[:rows] * shares[:, 0:1]
-            for k in range(1, top_count):
-                value = value + picked[k * rows : (k + 1) * rows] * shares[:, k : k + 1]
-            return value
-
-        def give_back(z, up):
-            share_copy(seq, z).wait_recv()
-            slot = z + up
-            outer = seq > 0 if up else seq + 1 < n_sp
-            for c in range(cols):
-                value = mixed(z, c)
-
-                @pl.when(outer)
+                span = slice(c * col_len, (c + 1) * col_len)
+                made = jnp.dot(hidden, down_w[:, span], preferred_element_type=F32).astype(BF16)
+                for i, z in enumerate(blocks):
+                    result[z, :, span] = made[i * plane_slots : (i + 1) * plane_slots]
+            for z in blocks:
+                for_mates(lambda peer: back_copy(z, peer).start())
+
+                @pl.when(z != seq)
                 def _():
-                    line_copy(z, c, up).wait_recv()
-                    line_out[z, c] = (value + line_in[slot, c].astype(F32)).astype(BF16)
-
-                @pl.when(jnp.logical_not(outer))
+                    back_copy(z, ten).start()
+
+                @pl.when(z == seq)
                 def _():
-                    line_out[z, c] = value.astype(BF16)
-
-                line_copy(z, c, up).start()
-
-        def chain(j):
-            @pl.when(n_sp - 1 - j < seq)
+                    returned[slot_ds(me), :] = result[z, slot_ds(ten), :]
+
+        def serve_pair(k):
+            low, high = seq - k - 1, seq + k
+            both = jnp.logical_and(low >= 0, high < n_sp)
+
+            if 2 * k + 1 < n_sp:
+
+                @pl.when(both)
+                def _():
+                    serve(low, high)
+
+            @pl.when(jnp.logical_not(both))
             def _():
-                give_back(n_sp - 1 - j, 0)
-
-            @pl.when(j > seq)
-            def _():
-                give_back(j, 1)
-
-        turn_choice(seq)
+                @pl.when(jnp.logical_or(low >= 0, high < n_sp))
+                def _():
+                    serve(jnp.where(low >= 0, low, high))
+
         squares = jnp.zeros((rows, 1), F32)
         gain = norm_gain[...].astype(F32).reshape(1, width)
         for c in range(cols):
@@ -625,80 +640,46 @@
             go_on(seq, c, 0)
             go_on(seq, c, 1)
             place_rows(seq, c)
+            take(0, c)
         lane_scale[seq] = scale_parts(squares)
         go_on(seq, cols, 0)
         go_on(seq, cols, 1)
         place_rows(seq, cols)
+        take(0, cols)
         for load in loads[2:]:
             load.wait()
+
+        def sent_own():
+            sent_plane(seq)
+            sent_lane(seq, 0)
+            sent_lane(seq, 1)
+
+        def sent_block(z, up):
+            sent_plane(z)
+            sent_lane(z, up)
 
         for step in range(1, n_sp + 2):
             moving = step < n_sp
             if moving:
                 take(step, 0)
-            if step == 2:
-                for c in range(cols):
-                    span = slice(c * col_len, (c + 1) * col_len)
-                    resid_ref[:, span] = resid_ref[:, span] + mixed(seq, c)
-            elif step > 2:
-                chain(step - 2)
             if moving:
                 take(step, 1)
-            if step == 1:
+            if step <= n_sp:
+                serve_pair(step - 1)
+            if moving:
                 for c in range(2, cols + 1):
                     take(step, c)
-                serve(seq)
-            elif step <= n_sp:
-                at_sides(step - 1, lambda z, up: serve(z))
-                if moving:
-                    for c in range(2, cols + 1):
-                        take(step, c)
-
-        for c in range(cols):
-            span = slice(c * col_len, (c + 1) * col_len)
-            for up in range(2):
-
-                @pl.when(seq > 0 if up else seq + 1 < n_sp)
-                def _():
-                    line_copy(seq, c, up).wait_recv()
-                    resid_ref[:, span] = resid_ref[:, span] + line_in[seq + up, c].astype(F32)
-
-            out[:, span] = resid_ref[:, span].astype(BF16)
-
-        for i in range(1, n_sp):
-            target = lax.rem(seq + i, n_sp)
-            pick_copy(target, seq).wait_send()
-            share_copy(target, seq).wait_send()
-
-        def sent_lane(z, c, up):
-            @pl.when(seq + 1 < n_sp if up else seq > 0)
-            def _():
-                lane_copy(z, c, up).wait_send()
-
-        def sent_block(z, carry):
-            for c in range(cols + 1):
-                for_mates(lambda peer: disp_copy(z, c, peer, ten).wait_send())
-                if c < cols:
-                    for_mates(lambda peer: back_copy(z, c, peer, ten).wait_send())
-                for up in range(2):
-
-                    @pl.when(z <= seq if up else z >= seq)
-                    def _():
-                        sent_lane(z, c, up)
-
-                if c < cols:
-
-                    @pl.when(z < seq)
-                    def _():
-                        line_copy(z, c, 0).wait_send()
-
-                    @pl.when(z > seq)
-                    def _():
-                        line_copy(z, c, 1).wait_send()
-
-            return carry
-
-        lax.fori_loop(0, n_sp, sent_block, 0)
+            if step > 1:
+                at_pair(step - 2, sent_block, sent_own)
+
+        others = pl.ds(0, (experts - 1) * cap)
+        bulk(
+            returned.at[others], returned.at[others], back_send.at[0], back_recv.at[0]
+        ).wait_recv()
+        finish()
+        bulk(
+            returned.at[others], returned.at[others], back_send.at[0], back_recv.at[0]
+        ).wait_send()
     else:
         def slot_ds(peer):
             return pl.ds(pl.multiple_of(peer * cap, cap), cap)
@@ -803,13 +784,7 @@
             return carry
 
         lax.fori_loop(1, experts, collect, 0)
-        for c in range(cols):
-            span = slice(c * col_len, (c + 1) * col_len)
-            picked = jnp.dot(pick_ref[...], returned[:, span], preferred_element_type=F32)
-            value = resid_ref[:, span]
-            for k in range(top_count):
-                value = value + picked[k * rows : (k + 1) * rows] * column(route_weight, k)
-            out[:, span] = value.astype(BF16)
+        finish()
 
         def sent_rows(i, carry):
             peer = lax.rem(me + i, experts)
@@ -826,17 +801,29 @@
         return carry
 
     lax.fori_loop(seq + 1, n_sp, sent_kv, 0)
+    if lined:
+
+        def sent_gates(target, carry):
+            gate_copy(seq, target, target).wait_send()
+            return carry
+
+        lax.fori_loop(0, seq, sent_gates, 0)
 
     def sent_fwd(block, carry):
-        for_mates(lambda peer: fwd_copy(block, ten, peer).wait_send())
+        pass_copy(block, pl.ds(0, n_tp - 1)).wait_send()
         return carry
 
     lax.fori_loop(0, seq, sent_fwd, 0)
-    for c in range(cols):
-        pair_copy(c).wait_send()
-        for hop in range(1, half_groups):
-            group = lax.rem(my_group + hop, half_groups)
-            cross_copy(c, group, my_group, hop).wait_send()
+    pltpu.make_async_remote_copy(
+        src_ref=pair_out,
+        dst_ref=pair_in,
+        send_sem=pair_send.at[0],
+        recv_sem=pair_recv.at[0],
+        device_id={"sp": seq, "tp": partner},
+        device_id_type=MESH,
+    ).wait_send()
+    for hop in range(1, half_groups):
+        cross_copy(pl.ds(0, cols), lax.rem(my_group + hop, half_groups), my_group, hop, 0).wait_send()
 
 
 def shards(
@@ -866,7 +853,7 @@
     size_small, size_large = key_small.shape[0], key_large.shape[0]
     heads_small, heads_large = forget_small.shape[0], forget_large.shape[0]
     heads = heads_small + heads_large
-    gate_rows = -(-heads // 8) * 8
+    gate_rows = -(-max(heads, 2 * top_count) // 8) * 8
     extra_rows = -(-3 * gate_rows // 16) * 16
     capacity = max(2, 2 * rows * top_count // experts)
     cap = -(-capacity // 16) * 16
@@ -881,32 +868,22 @@
     vmem, dma = pltpu.VMEM, pltpu.SemaphoreType.DMA
     if lined:
         tail = [
-            vmem((n_sp, top_count * rows, group), BF16),
-            vmem((n_sp, top_count * rows, group), BF16),
+            vmem((top_count * rows, slots), BF16),
             vmem((n_sp, group, rows), BF16),
-            vmem((n_sp, rows, 128), F32),
             vmem((n_sp, cols, rows, col_len), BF16),
             vmem((n_sp, rows, 128), BF16),
             vmem((n_sp, cols, group, col_len), BF16),
             vmem((n_sp, cols, group, col_len), BF16),
             vmem((n_sp, group, 128), BF16),
             vmem((n_sp, group, 128), BF16),
-            vmem((n_sp, cols, group, col_len), BF16),
-            vmem((n_sp, cols, group, col_len), BF16),
-            vmem((n_sp, cols, rows, col_len), BF16),
-            vmem((n_sp + 1, cols, rows, col_len), BF16),
-            dma((n_sp,)),
-            dma((n_sp,)),
-            dma((n_sp,)),
-            dma((n_sp,)),
-            dma((2, n_sp, cols + 1)),
+            vmem((n_sp, group, width), BF16),
+            vmem((slots, width), BF16),
+            dma((2, n_sp, 2)),
             dma((n_sp, cols + 1)),
-            dma((n_sp, cols + 1, n_tp)),
-            dma((n_sp, cols + 1, n_tp)),
-            dma((n_sp, cols, n_tp)),
-            dma((n_sp, cols, n_tp)),
-            dma((n_sp, cols)),
-            dma((n_sp + 1, cols)),
+            dma((n_sp, 2)),
+            dma((n_sp, cols + 1)),
+            dma((1,)),
+            dma((1,)),
         ]
     else:
         tail = [
@@ -930,7 +907,7 @@
         out_specs=pl.BlockSpec(memory_space=pltpu.VMEM),
         scratch_shapes=[
             vmem((n_sp, n_tp, 2 * (size_small + size_large) // n_tp, tokens), BF16),
-            vmem((n_sp, gate_rows, tokens), F32),
+            vmem((n_sp, gate_rows, tokens + -(-rows // 128) * 128), F32),
             vmem((heads_small, size_small + extra_rows, tokens), BF16),
             vmem((heads_large, size_large + extra_rows, tokens), BF16),
             vmem((gate_rows, tokens), F32),
@@ -954,11 +931,12 @@
             dma((n_sp,)),
             dma((n_sp,)),
             dma((n_sp,)),
-            dma((n_sp, n_tp)),
-            dma((n_sp, n_tp)),
+            dma((n_sp,)),
+            dma((n_sp, half_groups)),
+            dma((n_sp,)),
+            dma((1,)),
             dma((cols,)),
-            dma((cols,)),
-            dma((cols, half_groups)),
+            dma((half_groups,)),
             dma((cols, half_groups)),
         ]
         + tail,

time: 86.6 us -> 72.5 us (0.84)
  the two profiles are of different devices: /device:TPU:24 before, /device:TPU:0 now
where the time goes in v3:
time: 72.5 us; the launch traced here: 72.3 us
  Pallas kernels  70.7 us (98%)
  local copies, waits for them, and re-layouts  1.67 us (2%)
    pallas_call x1, Pallas kernels, shards(): pl.pallas_call(functools.partial(layer_kernel, (n_sp, n_tp, cap, col_len,...  70.7 us
    unnamed x1, local copies, waits for them, and re-layouts  1.67 us

profile of v3, /device:TPU:0, one launch (start us, length us, event | category | flops | bytes accessed | tf_op | source)
XLA Modules:
  0.0 72.3 jit_solution(13740971622999873389)
XLA Ops:
  0.0 70.7 %shard_map.163 = bf16[64,2048]{1,0:T(8,128)(2,1)} custom-call(bf16[64,2048]{1,0:T(8,128)(2,1)} %refs_0_.1, bf16[256,256]{1,0:T(8,128)(2,1)} %refs_1_.1, bf16[256,256]{1,0:T(8,128)(2,1)} %refs_2_.1, bf16[64,256]{1,0:T(8,128)(2,1)} %refs_3_.1, bf16[128,256]{1,0:T(8,128)(2,1)} %refs_4_.1, bf16[64,256]{1,0:T(8,128)(2,1)} %refs_5_.1, bf16[128,256]{1,0:T(8,128)(2,1)} %refs_6_.1, ...), custom_call_target="tpu_custom_call" | custom-call | tf_op jit(solution)/shard_map/pallas_call | solution.py:902
  70.7 1.7 %copy.19 = bf16[64,2048]{1,0:T(8,128)(2,1)} copy(bf16[64,2048]{1,0:T(8,128)(2,1)} %shard_map.163) | data formatting | bytes 524288

commit v4 on v3

--- a/solution.py
+++ b/solution.py
@@ -14,7 +14,14 @@
 
 
 def layer_kernel(dims, *refs):
+    given, refs = refs[:12], refs[12:]
     (
+        project_small,
+        project_large,
+        expert_gate,
+        expert_up,
+        expert_down,
+        out,
         residual_in,
         query_small,
         query_large,
@@ -27,12 +34,6 @@
         norm_gain,
         routing,
         route_weight,
-        project_small,
-        project_large,
-        expert_gate,
-        expert_up,
-        expert_down,
-        out,
         kv,
         gates,
         turned_q_small,
@@ -54,6 +55,7 @@
         cross_in,
         resid_ref,
         weight_sem,
+        given_sem,
         kv_send,
         kv_recv,
         gate_send,
@@ -68,6 +70,27 @@
         *tail,
     ) = refs
     n_sp, n_tp, cap, col_len, lined = dims
+    held = (
+        residual_in,
+        query_small,
+        query_large,
+        key_small,
+        key_large,
+        value_small,
+        value_large,
+        forget_small,
+        forget_large,
+        norm_gain,
+        routing,
+        route_weight,
+    )
+    fetches = [
+        pltpu.make_async_copy(source, target, given_sem.at[i])
+        for i, (source, target) in enumerate(zip(given, held))
+    ]
+    early, queries, late = (3, 4, 5, 6, 7, 8, 10, 11), (1, 2), (0, 9)
+    for i in early + queries + late:
+        fetches[i].start()
     experts = n_sp * n_tp
     seq = lax.axis_index("sp")
     ten = lax.axis_index("tp")
@@ -108,6 +131,8 @@
         return carry
 
     lax.fori_loop(1, experts, greet_all, 0)
+    for i in early:
+        fetches[i].wait()
 
     for p in range(n_tp):
         base = 0
@@ -177,7 +202,6 @@
             action(lax.rem(ten + i, n_tp))
 
     def send_kv(target, carry):
-        gate_copy(seq, target, target).start()
         kv_copy(seq, target, target).start()
         return carry
 
@@ -185,7 +209,8 @@
         gate_copy(seq, target, target).start()
         return carry
 
-    lax.fori_loop(seq + 1, n_sp, send_kv, 0)
+    lax.fori_loop(seq + 1, n_sp, send_gates, 0)
+    lax.fori_loop(seq + 1, jnp.minimum(seq + 2, n_sp), send_kv, 0)
     if lined:
         lax.fori_loop(0, seq, send_gates, 0)
     for load in loads:
@@ -265,12 +290,14 @@
     for k in range(top_count):
         pick_ref[k * rows : (k + 1) * rows, :] = (spots == places[k]).astype(F32).astype(BF16)
 
-    extra_rows = turned_q_small.shape[1] - size_small
+    extra_rows = turned_q_small.shape[0] - size_small
 
     def fold(size):
         power = 2.0 ** math.floor(math.log2(size**-0.5))
         return power, size**-0.5 / power
 
+    for i in queries:
+        fetches[i].wait()
     extra_row = lax.broadcasted_iota(jnp.int32, (extra_rows, tokens), 0)
     for kind in range(2):
         heads, size, offset, source, q_ref = (
@@ -280,17 +307,21 @@
         turned = (source[...] * fold(size)[0]).astype(BF16).T
         for h in range(heads):
             chosen = (lax.rem(extra_row, gate_rows) == offset + h) & (extra_row < 3 * gate_rows)
-            q_ref[h, :size, :] = turned[h * size : (h + 1) * size, :]
-            q_ref[h, size:, :] = jnp.where(chosen, 1.0, 0.0).astype(BF16)
+            span = slice(h * tokens, (h + 1) * tokens)
+            q_ref[:size, span] = turned[h * size : (h + 1) * size, :]
+            q_ref[size:, span] = jnp.where(chosen, 1.0, 0.0).astype(BF16)
     key_base = (0, piece_small)
     value_base = (piece_small + piece_large, 2 * piece_small + piece_large)
 
     def attend(block, diagonal):
         block_gates = gates[block][:, :tokens]
-        if diagonal:
-            k_pos = lax.broadcasted_iota(jnp.int32, (tokens, tokens), 0)
-            q_pos = lax.broadcasted_iota(jnp.int32, (tokens, tokens), 1)
-            seen = q_pos >= k_pos
+
+        def seen(heads):
+            shape = (tokens, heads * tokens)
+            k_pos = lax.broadcasted_iota(jnp.int32, shape, 0)
+            q_pos = lax.rem(lax.broadcasted_iota(jnp.int32, shape, 1), tokens)
+            return q_pos >= k_pos
+
         for kind in range(2):
             heads, size, piece, offset, q_ref, acc = (
                 (heads_small, size_small, piece_small, 0, turned_q_small, acc_small),
@@ -312,24 +343,23 @@
             values = jnp.concatenate(
                 [kv[block, p, vb : vb + piece, :] for p in range(n_tp)], axis=0
             )
-            for h in range(heads):
-                g = slice(offset + h, offset + h + 1)
-                scores = jnp.dot(keys, q_ref[h], preferred_element_type=F32)
-                if diagonal:
-                    scores = jnp.where(seen, scores, -jnp.inf)
-                block_top = jnp.max(scores, axis=0, keepdims=True)
-                top = block_top if diagonal else jnp.maximum(top_ref[g, :], block_top)
-                below_top = scores - top
-                weights = jnp.exp(below_top if rest == 1.0 else below_top * rest)
-                total = jnp.sum(weights, axis=0, keepdims=True)
-                mixed = jnp.dot(values, weights.astype(BF16), preferred_element_type=F32)
-                if not diagonal:
-                    factor = jnp.exp((top_ref[g, :] - top) * rest)
-                    total = total_ref[g, :] * factor + total
-                    mixed = acc[h] * factor + mixed
-                top_ref[g, :] = top
-                total_ref[g, :] = total
-                acc[h] = mixed
+            side = slice(offset * tokens, (offset + heads) * tokens)
+            scores = jnp.dot(keys, q_ref[...], preferred_element_type=F32)
+            if diagonal:
+                scores = jnp.where(seen(heads), scores, -jnp.inf)
+            block_top = jnp.max(scores, axis=0, keepdims=True)
+            top = block_top if diagonal else jnp.maximum(top_ref[:, side], block_top)
+            below_top = scores - top
+            weights = jnp.exp(below_top if rest == 1.0 else below_top * rest)
+            total = jnp.sum(weights, axis=0, keepdims=True)
+            mixed = jnp.dot(values, weights.astype(BF16), preferred_element_type=F32)
+            if not diagonal:
+                factor = jnp.exp((top_ref[:, side] - top) * rest)
+                total = total_ref[:, side] * factor + total
+                mixed = acc[...] * factor + mixed
+            top_ref[:, side] = top
+            total_ref[:, side] = total
+            acc[...] = mixed
 
     def share_out(block):
         kv_copy(block, seq, block).wait_recv()
@@ -344,16 +374,20 @@
             pass_copy(block, 2 * group + parity).start()
 
     attend(seq, True)
+    lax.fori_loop(seq + 2, n_sp, send_kv, 0)
+
+    def learn(distances):
+        if lined:
+            for i in distances:
+                z = lax.rem(seq + n_sp - i, n_sp)
+                gate_copy(z, seq, z).wait_recv()
+                prepare(z)
+
+    learn(range(1, n_sp))
 
     @pl.when(seq > 0)
     def _():
         share_out(seq - 1)
-
-    if lined:
-        for i in range(1, n_sp):
-            z = lax.rem(seq + i, n_sp)
-            gate_copy(z, seq, z).wait_recv()
-            prepare(z)
 
     def earlier_block(i, carry):
         @pl.when(i < seq)
@@ -377,14 +411,16 @@
     lax.fori_loop(1, jnp.where(seq > 0, seq + 2, 1), earlier_block, 0)
 
     for h in range(heads_small):
+        span = slice(h * tokens, (h + 1) * tokens)
         attn_t[h * size_small : (h + 1) * size_small, :] = (
-            acc_small[h] * (1.0 / total_ref[h : h + 1, :])
+            acc_small[:, span] * (1.0 / total_ref[:, span])
         ).astype(BF16)
     for h in range(heads_large):
         first = width_small + h * size_large
-        g = heads_small + h
+        span = slice(h * tokens, (h + 1) * tokens)
+        side = slice((heads_small + h) * tokens, (heads_small + h + 1) * tokens)
         attn_t[first : first + size_large, :] = (
-            acc_large[h] * (1.0 / total_ref[g : g + 1, :])
+            acc_large[:, span] * (1.0 / total_ref[:, side])
         ).astype(BF16)
     attn[...] = attn_t[...].T
 
@@ -413,6 +449,8 @@
 
     for load in loads[:2]:
         load.wait()
+    for i in late:
+        fetches[i].wait()
     for c in range(cols):
         part = jnp.dot(
             attn[...], proj_w[:, c * col_len : (c + 1) * col_len], preferred_element_type=F32
@@ -485,7 +523,7 @@
                 src_ref=source.at[slot_ds(peer)],
                 dst_ref=target.at[slot_ds(sender)],
                 send_sem=disp_send.at[z, 1 if c == cols else 0],
-                recv_sem=disp_recv.at[z, c],
+                recv_sem=disp_recv.at[z, 1 if c == cols else 0],
                 device_id={"sp": seq, "tp": peer},
                 device_id_type=MESH,
             )
@@ -513,9 +551,11 @@
                 device_id_type=MESH,
             )
 
-        def disp_came(z, c):
-            ref = arrived.at[z, c, mates_rows] if c < cols else scale_in.at[z, mates_rows]
-            bulk(ref, ref, disp_send.at[z, 0], disp_recv.at[z, c]).wait_recv()
+        def disp_came(z):
+            ref = arrived.at[z, :, mates_rows]
+            bulk(ref, ref, disp_send.at[z, 0], disp_recv.at[z, 0]).wait_recv()
+            ref = scale_in.at[z, mates_rows]
+            bulk(ref, ref, disp_send.at[z, 1], disp_recv.at[z, 1]).wait_recv()
 
         def sent_plane(z):
             ref = outgoing.at[z, :, mates_rows]
@@ -560,11 +600,6 @@
 
         def at_pair(k, action, own):
             low, high = seq - k - 1, seq + k
-
-            @pl.when(low >= 0)
-            def _():
-                action(low, 1)
-
             if k > 0:
 
                 @pl.when(high < n_sp)
@@ -573,6 +608,10 @@
             elif own is not None:
                 own()
 
+            @pl.when(low >= 0)
+            def _():
+                action(low, 1)
+
         def take(k, c):
             def one(z, up):
                 lane_copy(z, c, up).wait_recv()
@@ -582,18 +621,17 @@
             at_pair(k, one, None)
 
         def serve(*blocks):
-            count = len(blocks) * plane_slots
-            gate_part = jnp.zeros((count, gate_w.shape[1]), F32)
-            up_part = jnp.zeros((count, gate_w.shape[1]), F32)
-            for c in range(cols):
-                for z in blocks:
-                    disp_came(z, c)
-                came = jnp.concatenate([arrived[z, c] for z in blocks], axis=0)
-                depth = slice(c * col_len, (c + 1) * col_len)
-                gate_part = gate_part + jnp.dot(came, gate_w[depth, :], preferred_element_type=F32)
-                up_part = up_part + jnp.dot(came, up_w[depth, :], preferred_element_type=F32)
             for z in blocks:
-                disp_came(z, cols)
+                disp_came(z)
+            came = jnp.concatenate(
+                [
+                    jnp.concatenate([arrived[z, c] for c in range(cols)], axis=1)
+                    for z in blocks
+                ],
+                axis=0,
+            )
+            gate_part = jnp.dot(came, gate_w[...], preferred_element_type=F32)
+            up_part = jnp.dot(came, up_w[...], preferred_element_type=F32)
             row_scale = jnp.concatenate(
                 [jnp.sum(scale_in[z].astype(F32), axis=1, keepdims=True) for z in blocks], axis=0
             )
@@ -604,16 +642,14 @@
                 made = jnp.dot(hidden, down_w[:, span], preferred_element_type=F32).astype(BF16)
                 for i, z in enumerate(blocks):
                     result[z, :, span] = made[i * plane_slots : (i + 1) * plane_slots]
-            for z in blocks:
-                for_mates(lambda peer: back_copy(z, peer).start())
-
-                @pl.when(z != seq)
-                def _():
-                    back_copy(z, ten).start()
-
-                @pl.when(z == seq)
-                def _():
-                    returned[slot_ds(me), :] = result[z, slot_ds(ten), :]
+
+        def give(z, up):
+            for_mates(lambda peer: back_copy(z, peer).start())
+            back_copy(z, ten).start()
+
+        def give_own():
+            for_mates(lambda peer: back_copy(seq, peer).start())
+            returned[slot_ds(me), :] = result[seq, slot_ds(ten), :]
 
         def serve_pair(k):
             low, high = seq - k - 1, seq + k
@@ -623,7 +659,7 @@
 
                 @pl.when(both)
                 def _():
-                    serve(low, high)
+                    serve(high, low)
 
             @pl.when(jnp.logical_not(both))
             def _():
@@ -640,12 +676,12 @@
             go_on(seq, c, 0)
             go_on(seq, c, 1)
             place_rows(seq, c)
-            take(0, c)
         lane_scale[seq] = scale_parts(squares)
         go_on(seq, cols, 0)
         go_on(seq, cols, 1)
         place_rows(seq, cols)
-        take(0, cols)
+        for c in range(cols + 1):
+            take(0, c)
         for load in loads[2:]:
             load.wait()
 
@@ -661,14 +697,25 @@
         for step in range(1, n_sp + 2):
             moving = step < n_sp
             if moving:
-                take(step, 0)
-            if moving:
-                take(step, 1)
+                for c in range(cols + 1):
+                    take(step, c)
             if step <= n_sp:
                 serve_pair(step - 1)
-            if moving:
-                for c in range(2, cols + 1):
-                    take(step, c)
+                if step == 1:
+                    give_own()
+                else:
+
+                    @pl.when(seq + step - 1 < n_sp)
+                    def _():
+                        give(seq + step - 1, 0)
+
+            for earlier in range(1, min(step, n_sp) + 1):
+                due = jnp.maximum(earlier, n_sp - 1 - seq) == step
+
+                @pl.when(jnp.logical_and(due, seq >= earlier))
+                def _():
+                    give(seq - earlier, 1)
+
             if step > 1:
                 at_pair(step - 2, sent_block, sent_own)
 
@@ -866,6 +913,20 @@
     group = n_tp * cap
     lined = n_tp * capacity >= rows
     vmem, dma = pltpu.VMEM, pltpu.SemaphoreType.DMA
+    inputs = (
+        residual_in,
+        query_small,
+        query_large,
+        key_small,
+        key_large,
+        value_small,
+        value_large,
+        forget_small,
+        forget_large,
+        norm_gain,
+        routing.T,
+        route_weight.T,
+    )
     if lined:
         tail = [
             vmem((top_count * rows, slots), BF16),
@@ -881,7 +942,7 @@
             dma((2, n_sp, 2)),
             dma((n_sp, cols + 1)),
             dma((n_sp, 2)),
-            dma((n_sp, cols + 1)),
+            dma((n_sp, 2)),
             dma((1,)),
             dma((1,)),
         ]
@@ -902,18 +963,18 @@
     return pl.pallas_call(
         functools.partial(layer_kernel, (n_sp, n_tp, cap, col_len, lined)),
         out_shape=jax.ShapeDtypeStruct((rows, width), BF16),
-        in_specs=[pl.BlockSpec(memory_space=pltpu.VMEM)] * 12
-        + [pl.BlockSpec(memory_space=pl.ANY)] * 5,
+        in_specs=[pl.BlockSpec(memory_space=pl.ANY)] * 17,
         out_specs=pl.BlockSpec(memory_space=pltpu.VMEM),
-        scratch_shapes=[
+        scratch_shapes=[vmem(given.shape, given.dtype) for given in inputs]
+        + [
             vmem((n_sp, n_tp, 2 * (size_small + size_large) // n_tp, tokens), BF16),
             vmem((n_sp, gate_rows, tokens + -(-rows // 128) * 128), F32),
-            vmem((heads_small, size_small + extra_rows, tokens), BF16),
-            vmem((heads_large, size_large + extra_rows, tokens), BF16),
-            vmem((gate_rows, tokens), F32),
-            vmem((gate_rows, tokens), F32),
-            vmem((heads_small, size_small, tokens), F32),
-            vmem((heads_large, size_large, tokens), F32),
+            vmem((size_small + extra_rows, heads_small * tokens), BF16),
+            vmem((size_large + extra_rows, heads_large * tokens), BF16),
+            vmem((1, heads * tokens), F32),
+            vmem((1, heads * tokens), F32),
+            vmem((size_small, heads_small * tokens), F32),
+            vmem((size_large, heads_large * tokens), F32),
             vmem((attn_width, tokens), BF16),
             vmem((tokens, attn_width), BF16),
             vmem((attn_width, width), BF16),
@@ -927,6 +988,7 @@
             vmem((cols, half_groups, rows, col_len), BF16),
             vmem((rows, width), F32),
             dma((5,)),
+            dma((12,)),
             dma((n_sp,)),
             dma((n_sp,)),
             dma((n_sp,)),
@@ -944,18 +1006,7 @@
             collective_id=0, has_side_effects=True, vmem_limit_bytes=60 * 1024 * 1024
         ),
     )(
-        residual_in,
-        query_small,
-        query_large,
-        key_small,
-        key_large,
-        value_small,
-        value_large,
-        forget_small,
-        forget_large,
-        norm_gain,
-        routing.T,
-        route_weight.T,
+        *inputs,
         project_small,
         project_large,
         expert_gate,

time: 72.5 us -> 64.5 us (0.89)
  Pallas kernels: 70.7 us -> 62.7 us
    pallas_call x1, Pallas kernels: 70.7 us -> 62.7 us  [shards(): pl.pallas_call(functools.partial(layer_kernel, (n_sp, n_tp, cap, col_len,...]
where the time goes in v4:
time: 64.5 us; the launch traced here: 64.4 us
  Pallas kernels  62.7 us (97%)
  local copies, waits for them, and re-layouts  1.67 us (3%)
    pallas_call x1, Pallas kernels, shards(): pl.pallas_call(functools.partial(layer_kernel, (n_sp, n_tp, cap, col_len,...  62.7 us
    unnamed x1, local copies, waits for them, and re-layouts  1.67 us

profile of v4, /device:TPU:0, one launch (start us, length us, event | category | flops | bytes accessed | tf_op | source)
XLA Modules:
  0.0 64.4 jit_solution(578782333536655970)
XLA Ops:
  0.0 62.7 %shard_map.163 = bf16[64,2048]{1,0:T(8,128)(2,1)} custom-call(bf16[64,2048]{1,0:T(8,128)(2,1)} %refs_0_.1, bf16[256,256]{1,0:T(8,128)(2,1)} %refs_1_.1, bf16[256,256]{1,0:T(8,128)(2,1)} %refs_2_.1, bf16[64,256]{1,0:T(8,128)(2,1)} %refs_3_.1, bf16[128,256]{1,0:T(8,128)(2,1)} %refs_4_.1, bf16[64,256]{1,0:T(8,128)(2,1)} %refs_5_.1, bf16[128,256]{1,0:T(8,128)(2,1)} %refs_6_.1, ...), custom_call_target="tpu_custom_call" | custom-call | tf_op jit(solution)/shard_map/pallas_call | solution.py:963
  62.7 1.7 %copy.19 = bf16[64,2048]{1,0:T(8,128)(2,1)} copy(bf16[64,2048]{1,0:T(8,128)(2,1)} %shard_map.163) | data formatting | bytes 524288

commit v5 on v4

--- a/solution.py
+++ b/solution.py
@@ -61,7 +61,6 @@
         gate_send,
         gate_recv,
         share_send,
-        side_recv,
         pass_recv,
         pair_send,
         pair_recv,
@@ -102,7 +101,8 @@
     heads_small, heads_large = forget_small.shape[0], forget_large.shape[0]
     width_small = heads_small * size_small
     rows, width = residual_in.shape
-    piece_small, piece_large = size_small // n_tp, size_large // n_tp
+    piece_count = kv.shape[1]
+    piece_small, piece_large = size_small // piece_count, size_large // piece_count
     cols = width // col_len
     half_groups = n_tp // 2
     my_group = lax.div(ten, 2)
@@ -134,7 +134,7 @@
     for i in early:
         fetches[i].wait()
 
-    for p in range(n_tp):
+    for p in range(piece_count):
         base = 0
         for source, piece in (
             (key_small, piece_small),
@@ -155,8 +155,8 @@
 
     def kv_copy(source, target, slot):
         return pltpu.make_async_remote_copy(
-            src_ref=kv.at[source, ten],
-            dst_ref=kv.at[source, ten],
+            src_ref=kv.at[source, parity],
+            dst_ref=kv.at[source, parity],
             send_sem=kv_send.at[slot],
             recv_sem=kv_recv.at[source],
             device_id={"sp": target, "tp": ten},
@@ -170,20 +170,6 @@
             send_sem=gate_send.at[slot],
             recv_sem=gate_recv.at[source],
             device_id={"sp": target, "tp": ten},
-            device_id_type=MESH,
-        )
-
-    def other_group(hop):
-        return lax.rem(my_group + hop, half_groups)
-
-    def side_copy(source, group_from, group_to):
-        piece = kv.at[source, 2 * group_from + parity]
-        return pltpu.make_async_remote_copy(
-            src_ref=piece,
-            dst_ref=piece,
-            send_sem=share_send.at[source],
-            recv_sem=side_recv.at[source, group_from],
-            device_id={"sp": seq, "tp": 2 * group_to + parity},
             device_id_type=MESH,
         )
 
@@ -336,12 +322,12 @@
             if extra_rows > 3 * gate_rows:
                 pieces.append(jnp.zeros((extra_rows - 3 * gate_rows, tokens), F32))
             keys = jnp.concatenate(
-                [kv[block, p, kb : kb + piece, :] for p in range(n_tp)]
+                [kv[block, p, kb : kb + piece, :] for p in range(piece_count)]
                 + [jnp.concatenate(pieces, axis=0).astype(BF16)],
                 axis=0,
             ).T
             values = jnp.concatenate(
-                [kv[block, p, vb : vb + piece, :] for p in range(n_tp)], axis=0
+                [kv[block, p, vb : vb + piece, :] for p in range(piece_count)], axis=0
             )
             side = slice(offset * tokens, (offset + heads) * tokens)
             scores = jnp.dot(keys, q_ref[...], preferred_element_type=F32)
@@ -363,15 +349,7 @@
 
     def share_out(block):
         kv_copy(block, seq, block).wait_recv()
-        for hop in range(1, half_groups):
-            side_copy(block, my_group, other_group(hop)).start()
-        pass_copy(block, ten).start()
-
-    def hand_on(block):
-        for hop in range(1, half_groups):
-            group = other_group(hop)
-            side_copy(block, group, group).wait_recv()
-            pass_copy(block, 2 * group + parity).start()
+        pass_copy(block, parity).start()
 
     attend(seq, True)
     lax.fori_loop(seq + 2, n_sp, send_kv, 0)
@@ -385,30 +363,28 @@
 
     learn(range(1, n_sp))
 
-    @pl.when(seq > 0)
-    def _():
-        share_out(seq - 1)
+    def at_earlier(block):
+        @pl.when(block >= 0)
+        def _():
+            share_out(block)
+
+    at_earlier(seq - 1)
 
     def earlier_block(i, carry):
-        @pl.when(i < seq)
+        block = seq - i
+        pass_copy(block, 1 - parity).wait_recv()
+        if not lined:
+            gate_copy(block, seq, block).wait_recv()
+        attend(block, False)
+
+        @pl.when(jnp.logical_and(i == 1, seq > 1))
         def _():
-            share_out(seq - 1 - i)
-
-        @pl.when(i <= seq)
-        def _():
-            hand_on(seq - i)
-
-        @pl.when(i > 1)
-        def _():
-            block = seq + 1 - i
-            pass_copy(block, pl.ds(0, half_groups)).wait_recv()
-            if not lined:
-                gate_copy(block, seq, block).wait_recv()
-            attend(block, False)
-
+            share_out(seq - 2)
+
+        at_earlier(block - 2)
         return carry
 
-    lax.fori_loop(1, jnp.where(seq > 0, seq + 2, 1), earlier_block, 0)
+    lax.fori_loop(1, seq + 1, earlier_block, 0)
 
     for h in range(heads_small):
         span = slice(h * tokens, (h + 1) * tokens)
@@ -513,6 +489,8 @@
                 device_id_type=MESH,
             )
 
+        scale_out[...] = jnp.zeros(scale_out.shape, BF16)
+
         def disp_copy(z, c, peer, sender):
             source, target = (
                 (outgoing.at[z, c], arrived.at[z, c])
@@ -586,12 +564,15 @@
                     lane_copy(z, c, 0).start()
 
         def place_rows(z, c):
-            values = lane_rows[z, c] if c < cols else lane_scale[z]
-            placed = jnp.dot(choose[z], values, preferred_element_type=F32).astype(BF16)
             if c < cols:
-                outgoing[z, c] = placed
+                outgoing[z, c] = jnp.dot(
+                    choose[z], lane_rows[z, c], preferred_element_type=F32
+                ).astype(BF16)
             else:
-                scale_out[z] = placed
+                parts = lane_scale[z, :, :rows].astype(F32).T.astype(BF16)
+                scale_out[z, :, : parts.shape[1]] = jnp.dot(
+                    choose[z], parts, preferred_element_type=F32
+                ).astype(BF16)
             for_mates(lambda peer: disp_copy(z, c, peer, ten).start())
             if c < cols:
                 arrived[z, c, slot_ds(ten), :] = outgoing[z, c, slot_ds(ten), :]
@@ -618,7 +599,17 @@
                 go_on(z, c, up)
                 place_rows(z, c)
 
-            at_pair(k, one, None)
+            low, high = seq - k - 1, seq + k
+
+            @pl.when(low >= 0)
+            def _():
+                one(low, 1)
+
+            if k > 0:
+
+                @pl.when(high < n_sp)
+                def _():
+                    one(high, 0)
 
         def serve(*blocks):
             for z in blocks:
@@ -633,7 +624,13 @@
             gate_part = jnp.dot(came, gate_w[...], preferred_element_type=F32)
             up_part = jnp.dot(came, up_w[...], preferred_element_type=F32)
             row_scale = jnp.concatenate(
-                [jnp.sum(scale_in[z].astype(F32), axis=1, keepdims=True) for z in blocks], axis=0
+                [
+                    jnp.sum(
+                        scale_in[z, :, : lane_scale.shape[1]].astype(F32), axis=1, keepdims=True
+                    )
+                    for z in blocks
+                ],
+                axis=0,
             )
             gate_part, up_part = gate_part * row_scale, up_part * row_scale
             hidden = (gate_part / (1.0 + jnp.exp(-gate_part)) * up_part).astype(BF16)
@@ -676,7 +673,9 @@
             go_on(seq, c, 0)
             go_on(seq, c, 1)
             place_rows(seq, c)
-        lane_scale[seq] = scale_parts(squares)
+        lane_scale[seq] = jnp.zeros(lane_scale.shape[1:], BF16)
+        turned_scale = scale_parts(squares).astype(F32).T
+        lane_scale[seq, :, :rows] = turned_scale[: lane_scale.shape[1]].astype(BF16)
         go_on(seq, cols, 0)
         go_on(seq, cols, 1)
         place_rows(seq, cols)
@@ -701,9 +700,9 @@
                     take(step, c)
             if step <= n_sp:
                 serve_pair(step - 1)
-                if step == 1:
+                if step == n_sp:
                     give_own()
-                else:
+                if step > 1:
 
                     @pl.when(seq + step - 1 < n_sp)
                     def _():
@@ -857,7 +856,7 @@
         lax.fori_loop(0, seq, sent_gates, 0)
 
     def sent_fwd(block, carry):
-        pass_copy(block, pl.ds(0, n_tp - 1)).wait_send()
+        pass_copy(block, parity).wait_send()
         return carry
 
     lax.fori_loop(0, seq, sent_fwd, 0)
@@ -932,7 +931,7 @@
             vmem((top_count * rows, slots), BF16),
             vmem((n_sp, group, rows), BF16),
             vmem((n_sp, cols, rows, col_len), BF16),
-            vmem((n_sp, rows, 128), BF16),
+            vmem((n_sp, 16, -(-rows // 128) * 128), BF16),
             vmem((n_sp, cols, group, col_len), BF16),
             vmem((n_sp, cols, group, col_len), BF16),
             vmem((n_sp, group, 128), BF16),
@@ -967,7 +966,7 @@
         out_specs=pl.BlockSpec(memory_space=pltpu.VMEM),
         scratch_shapes=[vmem(given.shape, given.dtype) for given in inputs]
         + [
-            vmem((n_sp, n_tp, 2 * (size_small + size_large) // n_tp, tokens), BF16),
+            vmem((n_sp, 2, size_small + size_large, tokens), BF16),
             vmem((n_sp, gate_rows, tokens + -(-rows // 128) * 128), F32),
             vmem((size_small + extra_rows, heads_small * tokens), BF16),
             vmem((size_large + extra_rows, heads_large * tokens), BF16),
@@ -994,7 +993,6 @@
             dma((n_sp,)),
             dma((n_sp,)),
             dma((n_sp,)),
-            dma((n_sp, half_groups)),
             dma((n_sp,)),
             dma((1,)),
             dma((cols,)),

time: 64.5 us -> 63.7 us (0.988)
  Pallas kernels: 62.7 us -> 61.8 us
    pallas_call x1, Pallas kernels: 62.7 us -> 61.8 us  [shards(): pl.pallas_call(functools.partial(layer_kernel, (n_sp, n_tp, cap, col_len,...]
where the time goes in v5:
time: 63.7 us; the launch traced here: 63.5 us
  Pallas kernels  61.8 us (97%)
  local copies, waits for them, and re-layouts  1.67 us (3%)
    pallas_call x1, Pallas kernels, shards(): pl.pallas_call(functools.partial(layer_kernel, (n_sp, n_tp, cap, col_len,...  61.8 us
    unnamed x1, local copies, waits for them, and re-layouts  1.67 us

profile of v5, /device:TPU:0, one launch (start us, length us, event | category | flops | bytes accessed | tf_op | source)
XLA Modules:
  0.0 63.5 jit_solution(15033162915293146958)
XLA Ops:
  0.0 61.8 %shard_map.163 = bf16[64,2048]{1,0:T(8,128)(2,1)} custom-call(bf16[64,2048]{1,0:T(8,128)(2,1)} %refs_0_.1, bf16[256,256]{1,0:T(8,128)(2,1)} %refs_1_.1, bf16[256,256]{1,0:T(8,128)(2,1)} %refs_2_.1, bf16[64,256]{1,0:T(8,128)(2,1)} %refs_3_.1, bf16[128,256]{1,0:T(8,128)(2,1)} %refs_4_.1, bf16[64,256]{1,0:T(8,128)(2,1)} %refs_5_.1, bf16[128,256]{1,0:T(8,128)(2,1)} %refs_6_.1, ...), custom_call_target="tpu_custom_call" | custom-call | tf_op jit(solution)/shard_map/pallas_call | solution.py:962
  61.8 1.7 %copy.19 = bf16[64,2048]{1,0:T(8,128)(2,1)} copy(bf16[64,2048]{1,0:T(8,128)(2,1)} %shard_map.163) | data formatting | bytes 524288

commit v6 on v5

--- a/solution.py
+++ b/solution.py
@@ -961,7 +961,7 @@
         ]
     return pl.pallas_call(
         functools.partial(layer_kernel, (n_sp, n_tp, cap, col_len, lined)),
-        out_shape=jax.ShapeDtypeStruct((rows, width), BF16),
+        out_shape=pltpu.VMEM((rows, width), BF16),
         in_specs=[pl.BlockSpec(memory_space=pl.ANY)] * 17,
         out_specs=pl.BlockSpec(memory_space=pltpu.VMEM),
         scratch_shapes=[vmem(given.shape, given.dtype) for given in inputs]

time: 63.7 us -> 62 us (0.973)
  local copies, waits for them, and re-layouts: 1.67 us -> 0.71 us
  Pallas kernels: 61.8 us -> 61.1 us
    unnamed x1, local copies, waits for them, and re-layouts: 1.67 us -> 0.71 us
    pallas_call x1, Pallas kernels: 61.8 us -> 61.1 us  [shards(): pl.pallas_call(functools.partial(layer_kernel, (n_sp, n_tp, cap, col_len,...]
where the time goes in v6:
time: 62 us; the launch traced here: 61.9 us
  Pallas kernels  61.1 us (99%)
  local copies, waits for them, and re-layouts  0.71 us (1%)
    pallas_call x1, Pallas kernels, shards(): pl.pallas_call(functools.partial(layer_kernel, (n_sp, n_tp, cap, col_len,...  61.1 us

profile of v6, /device:TPU:0, one launch (start us, length us, event | category | flops | bytes accessed | tf_op | source)
XLA Modules:
  0.0 61.9 jit_solution(741952879879920481)
XLA Ops:
  0.0 61.1 %shard_map.163 = bf16[64,2048]{1,0:T(8,128)(2,1)S(1)} custom-call(bf16[64,2048]{1,0:T(8,128)(2,1)} %refs_0_.1, bf16[256,256]{1,0:T(8,128)(2,1)} %refs_1_.1, bf16[256,256]{1,0:T(8,128)(2,1)} %refs_2_.1, bf16[64,256]{1,0:T(8,128)(2,1)} %refs_3_.1, bf16[128,256]{1,0:T(8,128)(2,1)} %refs_4_.1, bf16[64,256]{1,0:T(8,128)(2,1)} %refs_5_.1, ...), custom_call_target="tpu_custom_call" | custom-call | tf_op jit(solution)/shard_map/pallas_call | solution.py:962
  61.2 0.7 %copy.19 = bf16[64,2048]{1,0:T(8,128)(2,1)} copy(bf16[64,2048]{1,0:T(8,128)(2,1)S(1)} %shard_map.163) | data formatting | bytes 524288

commit v7 on v6

--- a/solution.py
+++ b/solution.py
@@ -693,13 +693,24 @@
             sent_plane(z)
             sent_lane(z, up)
 
+        at_end = seq == 0
         for step in range(1, n_sp + 2):
             moving = step < n_sp
+            if step <= n_sp:
+
+                @pl.when(at_end)
+                def _():
+                    serve_pair(step - 1)
+
             if moving:
                 for c in range(cols + 1):
                     take(step, c)
             if step <= n_sp:
-                serve_pair(step - 1)
+
+                @pl.when(jnp.logical_not(at_end))
+                def _():
+                    serve_pair(step - 1)
+
                 if step == n_sp:
                     give_own()
                 if step > 1:

time: 62 us -> 62 us (level)
  no operation moved by 1% of the time
where the time goes in v7:
time: 62 us; the launch traced here: 61.9 us
  Pallas kernels  61.1 us (99%)
  local copies, waits for them, and re-layouts  0.71 us (1%)
    pallas_call x1, Pallas kernels, shards(): pl.pallas_call(functools.partial(layer_kernel, (n_sp, n_tp, cap, col_len,...  61.1 us

profile of v7, /device:TPU:0, one launch (start us, length us, event | category | flops | bytes accessed | tf_op | source)
XLA Modules:
  0.0 61.9 jit_solution(8727280968129456055)
XLA Ops:
  0.0 61.1 %shard_map.163 = bf16[64,2048]{1,0:T(8,128)(2,1)S(1)} custom-call(bf16[64,2048]{1,0:T(8,128)(2,1)} %refs_0_.1, bf16[256,256]{1,0:T(8,128)(2,1)} %refs_1_.1, bf16[256,256]{1,0:T(8,128)(2,1)} %refs_2_.1, bf16[64,256]{1,0:T(8,128)(2,1)} %refs_3_.1, bf16[128,256]{1,0:T(8,128)(2,1)} %refs_4_.1, bf16[64,256]{1,0:T(8,128)(2,1)} %refs_5_.1, ...), custom_call_target="tpu_custom_call" | custom-call | tf_op jit(solution)/shard_map/pallas_call | solution.py:973
  61.2 0.7 %copy.19 = bf16[64,2048]{1,0:T(8,128)(2,1)} copy(bf16[64,2048]{1,0:T(8,128)(2,1)S(1)} %shard_map.163) | data formatting | bytes 524288
